TPU v7x, 128 devices: a whole 4x4x4 slice. The times are simulated.
128 devices in a mesh: sp: 32 (over z, y, core), tp: 4 (over x).
Axes of the slice: x: 4, y: 4, z: 4, core: 2. Of those that a mesh axis runs over, the one named last changes fastest.
Arguments:
- residual: bfloat16 [8192, 2048], P('sp'), may hold values from -6 to 6
- queries: bfloat16 [8192, 8, 2, 128], P('sp', 'tp'), may hold values from -100 to 100
- key_rows: bfloat16 [8192, 8, 2, 128], P('sp', 'tp'), may hold values from -6 to 6
- values: bfloat16 [8192, 8, 256], P('sp', 'tp'), may hold values from -6 to 6
- lambda_head: float32 [8], P('tp'), may hold values from 0.3 to 0.8
- sub_gain: float32 [256], replicated, may hold values from 0.1 to 1.9
- w_out: bfloat16 [2048, 2048], P('tp'), may hold values from -0.125 to 0.125
- norm_gain: float32 [2048], replicated, may hold values from 0.1 to 1.9
- w_gate: bfloat16 [2048, 5632], P('sp', 'tp'), may hold values from -0.125 to 0.125
- w_up: bfloat16 [2048, 5632], P('sp', 'tp'), may hold values from -0.125 to 0.125
- conv_gate: float32 [3, 5632], P(None, 'tp'), may hold values from -3 to 3
- conv_up: float32 [3, 5632], P(None, 'tp'), may hold values from -3 to 3
- w_down: bfloat16 [5632, 2048], P('tp'), may hold values from -0.078125 to 0.078125
Outputs:
- layer_out: bfloat16 [8192, 2048], P(('sp', 'tp'))
All inputs are finite; a program needn't handle non-finite values.
Results may differ from a plain program's by a relative error of at most 0.017.
Values may be sent and summed in bfloat16 or wider, within the bound.
A program may use at most 192 MiB of HBM per device.

v0:
```python
import math

import jax
import jax.numpy as jnp
from jax import lax
from jax.sharding import PartitionSpec as P

epsilon = 1e-06
lambda_init = 0.8 - 0.6 * math.exp(-0.3)


def side_by_side(arrays, axis, dim, along):
    columns = [a.reshape(*a.shape[:along], -1) for a in arrays]
    both = jnp.concatenate(columns, axis=along)
    filled, at, done = (lax.all_gather(both, axis, axis=dim, tiled=True), 0, [])
    for a, column in zip(arrays, columns):
        share = filled[..., at : at + column.shape[along]]
        done.append(share.reshape(*share.shape[:along], *a.shape[along:]))
        at += column.shape[along]
    return tuple(done)


def split_up(array, dim, devices):
    before, after = (array.shape[:dim], array.shape[dim + 1 :])
    return jnp.moveaxis(array.reshape(*before, devices, -1, *after), dim, 0)


def sum_at_owner(array, axis, dim):
    blocks = split_up(array, dim, lax.axis_size(axis))
    arrived = lax.all_to_all(blocks, axis, split_axis=0, concat_axis=0, tiled=True)
    return arrived.astype(jnp.float32).sum(axis=0)


def laid_out(blocks, dim):
    dims = list(blocks.shape[1:])
    dims[dim] *= blocks.shape[0]
    return jnp.moveaxis(blocks, 0, dim).reshape(dims)


def copy_for_each(array, axis):
    devices = lax.axis_size(axis)
    return lax.all_to_all(
        jnp.broadcast_to(array[None], (devices, *array.shape)), axis, 0, 0, tiled=True
    )


def gather_directly(array, axis, dim):
    return laid_out(copy_for_each(array, axis), dim)


def in_one_piece(arrays, axis, dim, along):
    both = jnp.concatenate(arrays, axis=along)
    filled, at, done = (lax.all_gather(both, axis, axis=dim, tiled=True), 0, [])
    for a in arrays:
        done.append(lax.slice_in_dim(filled, at, at + a.shape[along], axis=along))
        at += a.shape[along]
    return tuple(done)


def from_behind(block, axis, distance):
    devices = range(lax.axis_size(axis))
    route = [(i - distance, i) for i in devices if i - distance in devices]
    return lax.ppermute(block, axis, route)


def row_norm(middle, norm_gain):
    row_square = jnp.mean(middle * middle, axis=-1, keepdims=True)
    return (middle * lax.rsqrt(row_square + epsilon) * norm_gain).astype(jnp.bfloat16)


def causal_mix(rows_in, prior_rows, taps):
    padded_rows = jnp.concatenate([prior_rows, rows_in], 0).astype(jnp.float32)
    return taps[0] * padded_rows[:-2] + taps[1] * padded_rows[1:-1] + taps[2] * padded_rows[2:]


def local(
    residual,
    queries,
    key_rows,
    values,
    lambda_head,
    sub_gain,
    w_out,
    norm_gain,
    w_gate,
    w_up,
    conv_gate,
    conv_up,
    w_down,
):
    tok_rows = queries.shape[0]
    head_count = queries.shape[1]
    val_width = values.shape[2]
    score_scale = 1.0 / math.sqrt(queries.shape[3])
    query_pos = lax.axis_index("sp") * tok_rows + jnp.arange(tok_rows, dtype=jnp.int32)
    run_max = jnp.full((head_count, 2, tok_rows), -1e30, jnp.float32)
    key_part, val_part = side_by_side((key_rows, values), "sp", 0, 2)
    key_pos = jnp.arange(key_part.shape[0], dtype=jnp.int32)
    causal_mask = key_pos[None, :] <= query_pos[:, None]
    scores = (
        jnp.einsum("qhcd,khcd->hcqk", queries, key_part, preferred_element_type=jnp.float32)
        * score_scale
    )
    scores = jnp.where(causal_mask, scores, -1e30)
    new_max = jnp.maximum(run_max, jnp.max(scores, axis=-1))
    weights = jnp.where(causal_mask, jnp.exp(scores - new_max[..., None]), 0.0)
    run_sum = jnp.sum(weights, axis=-1)
    run_acc = jnp.einsum(
        "hcqk,khe->hcqe", weights.astype(jnp.bfloat16), val_part, preferred_element_type=jnp.float32
    )
    run_max, run_sum, run_acc = (new_max, run_sum, run_acc)
    blended = run_acc / run_sum[..., None]
    attended = blended[:, 0] - lambda_head[:, None, None] * blended[:, 1]
    mean_square = jnp.mean(attended * attended, axis=-1, keepdims=True)
    normed = (attended * lax.rsqrt(mean_square + epsilon) * sub_gain * (1.0 - lambda_init)).astype(
        jnp.bfloat16
    )
    w_heads = w_out.reshape(head_count, val_width, w_out.shape[1])
    part_rows = tok_rows // lax.axis_size("tp")
    own_start = lax.axis_index("tp") * part_rows
    slab_rows = normed
    projected = sum_at_owner(
        jnp.einsum("hqe,hed->qd", slab_rows, w_heads, preferred_element_type=jnp.float32).astype(
            jnp.bfloat16
        ),
        "tp",
        0,
    )
    middle_own = (
        lax.dynamic_slice_in_dim(residual, own_start, part_rows, 0).astype(jnp.float32) + projected
    )
    gathered = gather_directly(row_norm(middle_own, norm_gain), "tp", 0)
    pieces = in_one_piece((w_gate, w_up), "sp", 0, 1)
    gate_pre = jnp.dot(gathered, pieces[0], preferred_element_type=jnp.float32)
    up_pre = jnp.dot(gathered, pieces[1], preferred_element_type=jnp.float32)
    gate_pre = gate_pre.astype(jnp.bfloat16)
    up_pre = up_pre.astype(jnp.bfloat16)
    prior_gate, prior_up = from_behind((gate_pre[-2:], up_pre[-2:]), "sp", 1)
    gate_mixed = causal_mix(gate_pre, prior_gate, conv_gate)
    up_mixed = causal_mix(up_pre, prior_up, conv_up)
    hidden = (jax.nn.silu(gate_mixed) * up_mixed).astype(jnp.bfloat16)
    slab_rows = hidden
    lowered = sum_at_owner(
        jnp.dot(slab_rows, w_down, preferred_element_type=jnp.float32).astype(jnp.bfloat16), "tp", 0
    )
    return (middle_own + lowered).astype(jnp.bfloat16)


def solution(mesh):
    placed = (
        P("sp", None),
        P("sp", "tp", None, None),
        P("sp", "tp", None, None),
        P("sp", "tp", None),
        P("tp"),
        P(),
        P("tp", None),
        P(),
        P("sp", "tp"),
        P("sp", "tp"),
        P(None, "tp"),
        P(None, "tp"),
        P("tp", None),
    )
    return jax.shard_map(
        local, mesh=mesh, in_specs=placed, out_specs=P(("sp", "tp"), None), check_vma=False
    )
```

profile of v0, /device:TPU:1, one launch (start us, length us, event | category | flops | bytes accessed | tf_op | source)
XLA Modules:
  0.0 243.1 jit_solution(13935810480938369836)
XLA Ops:
  6.5 1.3 copy.20
  7.8 1.1 copy.21
  10.6 2.8 %iota_compare_fusion = pred[256,8192]{0,1:T(8,128)(4,1)} fusion(s32[256]{0:T(256)S(1)} %iota_add_fusion), kind=kLoop, calls=%fused_computation.8 | loop fusion | flops 2097152 | bytes 2098176 | tf_op jit(solution)/shard_map/le | solution.py:99
  13.4 80.2 %all-gather.3.cloned.1.call-done = bf16[8192,2,512]{0,2,1:T(8,128)(2,1)} async-done(((bf16[256,2,512]{0,2,1:T(8,128)(2,1)}), bf16[8192,2,512]{0,2,1:T(8,128)(2,1)}) %all-gather.3.cloned.1.call-update) | async-done | bytes 16777232 | tf_op jit(solution)/shard_map/all_gather | solution.py:15
  93.6 7.6 %slice.81 = bf16[8192,2,256]{0,2,1:T(8,128)(2,1)} slice(bf16[8192,2,512]{0,2,1:T(8,128)(2,1)} %all-gather.3.cloned.1.call-done), slice={[0:8192], [0:2], [0:256]} | slice | bytes 16777216 | tf_op jit(solution)/shard_map/slice | solution.py:17
  101.3 16.8 %fusion = (f32[2,2,256]{2,1,0:T(2,128)S(1)}, f32[2,2,8192,256]{3,2,1,0:T(8,128)}) fusion(pred[256,8192]{0,1:T(8,128)(4,1)} %iota_compare_fusion, bf16[8192,2,2,128]{0,3,2,1:T(8,128)(2,1)} %bitcast.58, bf16[256,2,2,128]{3,2,1,0:T(2,128)(2,1)S(1)} %copy-done.8), kind=kOutput, calls=%fused_computation.2 | convolution fusion | flops 2172648448 | bytes 44306432 | tf_op jit(solution)/shard_map/qhcd,khcd->hcqk/dot_general | solution.py:101
  118.0 15.7 %fusion.1 = f32[2,2,256]{2,1,0:T(2,128)S(1)} fusion(f32[2,2,8192,256]{3,2,1,0:T(8,128)} %get-tuple-element.12, f32[2,2,256]{2,1,0:T(2,128)S(1)} %broadcast_maximum_fusion, pred[256,8192]{0,1:T(8,128)(4,1)} %iota_compare_fusion), kind=kLoop, calls=%fused_computation.3 | loop fusion | flops 41942016 | bytes 35659776 | tf_op jit(solution)/shard_map/reduce_sum | solution.py:107
  133.7 18.3 %fusion.23 = f32[2,2,256,256]{2,3,1,0:T(8,128)S(1)} fusion(f32[2,2,8192,256]{3,2,1,0:T(8,128)} %get-tuple-element.12, f32[2,2,256]{2,1,0:T(2,128)S(1)} %broadcast_maximum_fusion, pred[256,8192]{0,1:T(8,128)(4,1)} %iota_compare_fusion, bf16[8192,2,512]{0,2,1:T(8,128)(2,1)} %all-gather.3.cloned.1.call-done, f32[2,2,256]{2,1,0:T(2,128)S(1)} %fusion.1), kind=kOutput, calls=%fused_computation.32 | convolution fusion | flops 4337172480 | bytes 45096960 | tf_op jit(solution)/shard_map/hcqk,khe->hcqe/dot_general | solution.py:108
  152.2 1.9 fusion.10
  154.1 4.4 %all-to-all-start = ((bf16[4,64,2048]{2,1,0:T(8,128)(2,1)}), bf16[4,64,2048]{2,1,0:T(8,128)(2,1)}, u32[]{:S(2)}, u32[]{:S(2)}) async-start(bf16[4,64,2048]{2,1,0:T(8,128)(2,1)} %bitcast.9), calls=%async_computation | async-start | bytes 2097152 | tf_op jit(solution)/shard_map/all_to_all | solution.py:30
  158.5 14.9 %all-to-all-done = bf16[4,64,2048]{2,1,0:T(8,128)(2,1)} async-done(((bf16[4,64,2048]{2,1,0:T(8,128)(2,1)}), bf16[4,64,2048]{2,1,0:T(8,128)(2,1)}, u32[]{:S(2)}, u32[]{:S(2)}) %all-to-all-start) | async-done | bytes 1048608 | tf_op jit(solution)/shard_map/all_to_all | solution.py:30
  173.4 1.4 convert_reduce_fusion.1
  174.8 1.1 multiply_reduce_fusion
  176.0 1.1 multiply_convert_fusion
  177.1 1.2 broadcast_in_dim.34
  178.2 4.4 %all-to-all-start.1 = ((bf16[4,64,2048]{2,1,0:T(8,128)(2,1)}), bf16[4,64,2048]{2,1,0:T(8,128)(2,1)}, u32[]{:S(2)}, u32[]{:S(2)}) async-start(bf16[4,64,2048]{2,1,0:T(8,128)(2,1)} %broadcast_in_dim.34), calls=%async_computation.1 | async-start | bytes 2097152 | tf_op jit(solution)/shard_map/all_to_all | solution.py:42
  182.8 13.7 %all-to-all-done.1 = bf16[4,64,2048]{2,1,0:T(8,128)(2,1)} async-done(((bf16[4,64,2048]{2,1,0:T(8,128)(2,1)}), bf16[4,64,2048]{2,1,0:T(8,128)(2,1)}, u32[]{:S(2)}, u32[]{:S(2)}) %all-to-all-start.1) | async-done | bytes 1048608 | tf_op jit(solution)/shard_map/all_to_all | solution.py:42
  196.5 4.8 %fusion.11 = bf16[256,1408]{1,0:T(8,128)(2,1)S(1)} fusion(bf16[256,2048]{1,0:T(8,128)(2,1)} %bitcast.10, bf16[2048,2816]{1,0:T(8,128)(2,1)} %all-gather.5.cloned.1.call-done), kind=kOutput, calls=%fused_computation.15 | convolution fusion | flops 1476755456 | bytes 7536640 | tf_op jit(solution)/shard_map/dot_general | solution.py:134
  201.3 5.0 %collective-permute-start = (bf16[2,1408]{1,0:T(2,128)(2,1)S(1)}, bf16[2,1408]{1,0:T(2,128)(2,1)S(1)}, u32[]{:S(2)}, u32[]{:S(2)}) collective-permute-start(bf16[2,1408]{1,0:T(2,128)(2,1)S(1)} %slice.85), channel_id=1, source_target_pairs={{0,4},{4,8},{8,12},{12,16},{16,20},{20,24},{24,28},{28,32},{32,36}... | collective-permute-start | bytes 16904 | tf_op jit(solution)/shard_map/ppermute | solution.py:63
  206.3 4.8 %fusion.14 = bf16[256,1408]{1,0:T(8,128)(2,1)S(1)} fusion(bf16[256,2048]{1,0:T(8,128)(2,1)} %bitcast.10, bf16[2048,2816]{1,0:T(8,128)(2,1)} %all-gather.5.cloned.1.call-done), kind=kOutput, calls=%fused_computation.16 | convolution fusion | flops 1476755456 | bytes 7536640 | tf_op jit(solution)/shard_map/dot_general | solution.py:135
  211.1 2.1 collective-permute-start.1
  214.4 2.6 %convolution_convert_fusion = bf16[256,2048]{1,0:T(8,128)(2,1)S(1)} fusion(bf16[1408,2048]{1,0:T(8,128)(2,1)S(1)} %bitcast.62, f32[258,1408]{1,0:T(8,128)S(1)} %maximum_convert_fusion.1, f32[258,1408]{1,0:T(8,128)S(1)} %maximum_convert_fusion, f32[1408]{0:T(1024)S(1)} %get-tuple-element.9, f32[1408]{0:T(1024)S(1)} %get-tuple-element.10, ...), kind=kOutput, calls=%fused_computation.17 | convolution fusion | flops 1482686464 | bytes 15515648 | tf_op jit(solution)/shard_map/dot_general | solution.py:144
  217.0 17.3 %all_to_all.15 = bf16[4,64,2048]{2,1,0:T(8,128)(2,1)S(1)} all-to-all(bf16[4,64,2048]{2,1,0:T(8,128)(2,1)S(1)} %bitcast.59), channel_id=1, replica_groups=mesh['sp'=32,'tp'=4] {'tp'}, dimensions={0} | all-to-all | bytes 2097152 | tf_op jit(solution)/shard_map/all_to_all | solution.py:30
  234.5 1.7 add_convert_fusion
  (43 shorter events, 3.3 us)
Async XLA Ops:
  6.5 145.7 %copy-start = (bf16[512,2048]{1,0:T(8,128)(2,1)S(1)}, bf16[512,2048]{1,0:T(8,128)(2,1)}, u32[]{:S(2)}) copy-start(bf16[512,2048]{1,0:T(8,128)(2,1)} %param.19) | copy-start | bytes 6291460
  6.5 3.3 %copy-start.2 = (bf16[64,1408]{1,0:T(8,128)(2,1)S(1)}, bf16[64,1408]{1,0:T(8,128)(2,1)}, u32[]{:S(2)}) copy-start(bf16[64,1408]{1,0:T(8,128)(2,1)} %param.21) | copy-start | bytes 540676
  6.5 3.3 %copy-start.1 = (bf16[64,1408]{1,0:T(8,128)(2,1)S(1)}, bf16[64,1408]{1,0:T(8,128)(2,1)}, u32[]{:S(2)}) copy-start(bf16[64,1408]{1,0:T(8,128)(2,1)} %param.22) | copy-start | bytes 540676
  6.5 87.1 %all-gather.3.cloned.1.call-start = ((), (), s32[]{:S(2)}) async-start(), calls=%async_computation.3 | async-start | bytes 17301504 | tf_op jit(solution)/shard_map/all_gather | solution.py:15
  9.8 173.0 %all-gather.5.cloned.1.call-start = ((), (), s32[]{:S(2)}) async-start(), calls=%async_computation.4 | async-start | bytes 11894784 | tf_op jit(solution)/shard_map/all_gather | solution.py:53
  13.4 87.8 %copy-start.8 = (bf16[256,2,2,128]{3,2,1,0:T(2,128)(2,1)S(1)}, bf16[256,2,2,128]{3,2,1,0:T(2,128)(2,1)}, u32[]{:S(2)}) copy-start(bf16[256,2,2,128]{3,2,1,0:T(2,128)(2,1)} %param.14) | copy-start | bytes 786436
  133.7 18.3 %copy-start.6 = (f32[2]{0:T(128)S(1)}, f32[2]{0:T(128)}, u32[]{:S(2)}) copy-start(f32[2]{0:T(128)} %param.17) | copy-start | bytes 28
  133.7 18.5 %copy-start.7 = (f32[256]{0:T(256)S(1)}, f32[256]{0:T(256)}, u32[]{:S(2)}) copy-start(f32[256]{0:T(256)} %param.18) | copy-start | bytes 3076
  154.1 21.9 %copy-start.5 = (f32[2048]{0:T(1024)S(1)}, f32[2048]{0:T(1024)}, u32[]{:S(2)}) copy-start(f32[2048]{0:T(1024)} %param.20) | copy-start | bytes 24580
  154.1 19.3 %all-to-all-start = ((bf16[4,64,2048]{2,1,0:T(8,128)(2,1)}), bf16[4,64,2048]{2,1,0:T(8,128)(2,1)}, u32[]{:S(2)}, u32[]{:S(2)}) async-start(bf16[4,64,2048]{2,1,0:T(8,128)(2,1)} %bitcast.9), calls=%async_computation | async-start | bytes 2097152 | tf_op jit(solution)/shard_map/all_to_all | solution.py:30
  176.0 6.7 %copy-start.3 = (f32[3,1408]{1,0:T(4,128)S(1)}, f32[3,1408]{1,0:T(4,128)}, u32[]{:S(2)}) copy-start(f32[3,1408]{1,0:T(4,128)} %param.24) | copy-start | bytes 50692
  176.0 6.7 %copy-start.4 = (f32[3,1408]{1,0:T(4,128)S(1)}, f32[3,1408]{1,0:T(4,128)}, u32[]{:S(2)}) copy-start(f32[3,1408]{1,0:T(4,128)} %param.23) | copy-start | bytes 50692
  178.2 18.3 %all-to-all-start.1 = ((bf16[4,64,2048]{2,1,0:T(8,128)(2,1)}), bf16[4,64,2048]{2,1,0:T(8,128)(2,1)}, u32[]{:S(2)}, u32[]{:S(2)}) async-start(bf16[4,64,2048]{2,1,0:T(8,128)(2,1)} %broadcast_in_dim.34), calls=%async_computation.1 | async-start | bytes 2097152 | tf_op jit(solution)/shard_map/all_to_all | solution.py:42
  201.3 13.1 %slice-start = ((s8[5767168]{0:T(1024)(128)(4,1)}), s8[4194304]{0:T(1024)(128)(4,1)S(1)}, s32[]{:S(2)}) async-start(s8[5767168]{0:T(1024)(128)(4,1)} %bitcast.61), calls=%async_computation.5 | async-start | bytes 8388608
  201.3 13.0 %slice-start.1 = ((s8[5767168]{0:T(1024)(128)(4,1)}), s8[1572864]{0:T(1024)(128)(4,1)S(1)}, s32[]{:S(2)}) async-start(s8[5767168]{0:T(1024)(128)(4,1)} %bitcast.61), calls=%async_computation.6 | async-start | bytes 3145728
  201.3 11.9 %collective-permute-start = (bf16[2,1408]{1,0:T(2,128)(2,1)S(1)}, bf16[2,1408]{1,0:T(2,128)(2,1)S(1)}, u32[]{:S(2)}, u32[]{:S(2)}) collective-permute-start(bf16[2,1408]{1,0:T(2,128)(2,1)S(1)} %slice.85), channel_id=1, source_target_pairs={{0,4},{4,8},{8,12},{12,16},{16,20},{20,24},{24,28},{28,32},{32,36}... | collective-permute-start | bytes 16904 | tf_op jit(solution)/shard_map/ppermute | solution.py:63
  211.1 3.1 %collective-permute-start.1 = (bf16[2,1408]{1,0:T(2,128)(2,1)S(1)}, bf16[2,1408]{1,0:T(2,128)(2,1)S(1)}, u32[]{:S(2)}, u32[]{:S(2)}) collective-permute-start(bf16[2,1408]{1,0:T(2,128)(2,1)S(1)} %slice.90), channel_id=1, source_target_pairs={{0,4},{4,8},{8,12},{12,16},{16,20},{20,24},{24,28},{28,32},{32,36}... | collective-permute-start | bytes 16904 | tf_op jit(solution)/shard_map/ppermute | solution.py:63
Sparse Core Ops, SparseCore 0:
  9.9 83.7 all-gather.2
  95.9 60.3 all-gather.4
where the time goes:
time: 244 us; the launch traced here: 243 us
  waiting for transfers between devices  110 us (45%)
  matrix products  49.1 us (20%)
  other arithmetic  26 us (11%)
  blocking collectives  17.3 us (7%)
  starting transfers between devices  15.9 us (7%)
  between operations  13.7 us (6%)
  local copies, waits for them, and re-layouts  11.3 us (5%)
    all_gather x1, waiting for transfers between devices, side_by_side(): filled, at, done = (lax.all_gather(both, axis, axis=dim, tiled=True), 0, [])  80.2 us
    dot_general x1, matrix products, local(): jnp.einsum('hcqk,khe->hcqe', weights.astype(jnp.bfloat16), val_part, pref...  18.3 us
    all_to_all x1, blocking collectives, sum_at_owner(): lax.all_to_all(blocks, axis, split_axis=0, concat_axis=0, tiled=True)  17.3 us
    dot_general x1, matrix products, local(): jnp.einsum('qhcd,khcd->hcqk', queries, key_part, preferred_element_type=j...  16.8 us
    reduce_sum x1, other arithmetic, local(): run_sum = jnp.sum(weights, axis=-1)  15.7 us
    all_to_all x1, waiting for transfers between devices, sum_at_owner(): lax.all_to_all(blocks, axis, split_axis=0, concat_axis=0, tiled=True)  14.9 us
    all_to_all x1, waiting for transfers between devices, copy_for_each(): lax.all_to_all(jnp.broadcast_to(array[None], (devices, *array.shape)), ax...  13.7 us
    slice x1, local copies, waits for them, and re-layouts, side_by_side(): share = filled[..., at:at + column.shape[along]]  7.62 us
  transfers between devices with their start and end apart: 6, of which 4 were waited for; matrix products, arithmetic and copies ran while one was open for 30% of the time, Pallas kernels for 0%

commit v1 on v0

v1 whole, which is shorter than its diff:
```python
import functools
import math

import jax
import jax.numpy as jnp
from jax import lax
from jax.experimental import pallas as pl
from jax.experimental.pallas import tpu as pltpu
from jax.sharding import PartitionSpec as P

EPS = 1e-06
LAMBDA_INIT = 0.8 - 0.6 * math.exp(-0.3)
BF16, F32 = jnp.bfloat16, jnp.float32
MESH = pl.DeviceIdType.MESH

ORDER = (
    (0, 0),
    (1, 0), (3, 0), (0, 1), (0, 3),
    (1, 1), (1, 3), (3, 1), (3, 3),
    (2, 0), (0, 2),
    (2, 1), (2, 3), (1, 2), (3, 2),
    (2, 2),
)
STEP_OF = {d: t for t, d in enumerate(ORDER)}
FIRST = (0, 1, 3, 2)


def pick(t, values):
    return sum(jnp.where(t == i, v, 0) for i, v in enumerate(values) if v)


class Where:
    def __init__(self):
        self.sp = lax.axis_index("sp")
        self.x = lax.axis_index("tp")
        self.core = lax.rem(self.sp, 2)
        self.chip = self.sp // 2
        self.y = lax.rem(self.chip, 4)
        self.z = self.chip // 4

    def chip_behind(self, dy, dz):
        return lax.rem(self.z + 4 - dz, 4) * 4 + lax.rem(self.y + 4 - dy, 4)


class Gather:
    def __init__(self, at, buf, first, base, send, recv, dsend, drecv):
        self.at, self.buf, self.first, self.base = at, buf, first, base
        self.send, self.recv, self.dsend, self.drecv = send, recv, dsend, drecv
        self.half = buf.shape[1] // 2

    def disp(self, df, dg):
        return (df, dg) if self.first == "y" else (dg, df)

    def slot(self, df, dg):
        return self.at.chip_behind(*self.disp(df, dg)) * 2 + self.at.core

    def neighbour(self, axis, step):
        d = {1: 3, -1: 1}[step]
        return self.slot(d, 0) if axis == "f" else self.slot(0, d)

    def copy(self, ident, slot, half, to):
        ref = self.buf.at[slot]
        if half is not None:
            ref = self.buf.at[slot, pl.ds(half * self.half, self.half)]
        return pltpu.make_async_remote_copy(
            src_ref=ref, dst_ref=ref,
            send_sem=self.send.at[self.base + ident], recv_sem=self.recv.at[self.base + ident],
            device_id={"sp": to}, device_id_type=MESH,
        )

    def out(self, ident, df, dg, half, axis, step):
        self.copy(ident, self.slot(df, dg), half, self.neighbour(axis, step)).start()

    def into(self, ident, df, dg, half=None):
        self.copy(ident, self.slot(df, dg), half, self.at.sp).wait_recv()

    def across(self, df, dg):
        t = STEP_OF[self.disp(df, dg)]
        ref = self.buf.at[self.slot(df, dg)]
        self.over(t, ref).start()

    def over(self, t, ref):
        other = self.at.sp + 1 - 2 * self.at.core
        return pltpu.make_async_remote_copy(
            src_ref=ref, dst_ref=ref, send_sem=self.dsend.at[t], recv_sem=self.drecv.at[t],
            device_id={"sp": other}, device_id_type=MESH,
        )

    def from_other(self, t, chip):
        self.over(t, self.buf.at[chip * 2 + 1 - self.at.core]).wait_recv()

    def start(self):
        self.out(0, 0, 0, None, "f", 1)
        self.out(1, 0, 0, None, "f", -1)
        self.across(0, 0)
        self.out(4, 0, 0, None, "g", 1)
        self.out(5, 0, 0, None, "g", -1)

    def along_second(self, j):
        self.out(4 + 4 * j, FIRST[j], 0, None, "g", 1)
        self.out(5 + 4 * j, FIRST[j], 0, None, "g", -1)
        self.across(FIRST[j], 0)

    def got_first(self):
        self.into(0, 1, 0)
        self.out(2, 1, 0, 0, "f", 1)
        self.along_second(1)
        self.into(1, 3, 0)
        self.out(3, 3, 0, 1, "f", -1)
        self.along_second(2)

    def got_second(self, j):
        self.into(4 + 4 * j, FIRST[j], 1)
        self.out(6 + 4 * j, FIRST[j], 1, 0, "g", 1)
        self.across(FIRST[j], 1)
        self.into(5 + 4 * j, FIRST[j], 3)
        self.out(7 + 4 * j, FIRST[j], 3, 1, "g", -1)
        self.across(FIRST[j], 3)

    def got_opposite(self):
        self.into(2, 2, 0, 0)
        self.into(3, 2, 0, 1)
        self.along_second(3)

    def got_far(self, j):
        self.into(6 + 4 * j, FIRST[j], 2, 0)
        self.into(7 + 4 * j, FIRST[j], 2, 1)
        self.across(FIRST[j], 2)

    def drain(self):
        for ident in range(20):
            half = 0 if ident % 4 >= 2 else None
            self.copy(ident, self.at.sp, half, self.at.sp).wait_send()
        for t in range(16):
            self.over(t, self.buf.at[self.at.sp]).wait_send()


def kernel(
    lam, sub_gain, norm_gain, conv_g, conv_u,
    q_in, k_in, v_in, wg_in, wu_in, wo_in, wd_in, res_in,
    out,
    q, kbuf, vbuf, wg, wu, wo, wd, res,
    m_s, l_s, acc, n_loc, n_all, mid, hn, hid, head, tail, halo, part, parts,
    lsem, send, recv, dsend, drecv, xsend, xrecv, psend, precv,
):
    at = Where()
    x, sp, core = at.x, at.sp, at.core
    rows = q.shape[0]
    own = rows // 4

    loads = [
        pltpu.make_async_copy(src, dst, lsem.at[i])
        for i, (src, dst) in enumerate(
            (
                (k_in, kbuf.at[sp]), (v_in, vbuf.at[sp]), (q_in, q), (wo_in, wo.at[x]), (wg_in, wg.at[sp]),
                (wu_in, wu.at[sp]), (wd_in, wd), (res_in.at[pl.ds(x * own, own)], res),
            )
        )
    ]
    for load in loads:
        load.start()

    barrier = pltpu.get_barrier_semaphore()
    other = sp + 1 - 2 * core
    y_up, y_down = at.chip_behind(3, 0) * 2 + core, at.chip_behind(1, 0) * 2 + core
    z_up, z_down = at.chip_behind(0, 3) * 2 + core, at.chip_behind(0, 1) * 2 + core
    after, before = lax.rem(sp + 1, 32), lax.rem(sp + 31, 32)
    for to in (other, y_up, y_down, z_up, z_down, after, before):
        pl.semaphore_signal(barrier, inc=1, device_id={"sp": to}, device_id_type=MESH)
    xs = [lax.rem(x + d, 4) for d in range(4)]
    for to in xs[1:]:
        pl.semaphore_signal(barrier, inc=1, device_id={"tp": to}, device_id_type=MESH)
    pl.semaphore_wait(barrier, 10)

    keys = Gather(at, kbuf, "y", 0, send, recv, dsend.at[0], drecv.at[0])
    vals = Gather(at, vbuf, "z", 20, send, recv, dsend.at[1], drecv.at[1])
    gate = Gather(at, wg, "y", 40, send, recv, dsend.at[2], drecv.at[2])
    up = Gather(at, wu, "z", 60, send, recv, dsend.at[3], drecv.at[3])

    loads[0].wait()
    keys.start()
    loads[1].wait()
    vals.start()

    wo_half = wo.shape[1] // 2
    wo_rows = core * wo_half

    def wo_copy(ident, slot, start, size, to):
        ref = wo.at[slot, pl.ds(wo_rows + start, size)]
        return pltpu.make_async_remote_copy(
            src_ref=ref, dst_ref=ref, send_sem=xsend.at[ident], recv_sem=xrecv.at[ident],
            device_id={"tp": to}, device_id_type=MESH,
        )

    def wo_over(ident, slot, which):
        ref = wo.at[slot, pl.ds(which * wo_half, wo_half)]
        return pltpu.make_async_remote_copy(
            src_ref=ref, dst_ref=ref, send_sem=xsend.at[ident], recv_sem=xrecv.at[ident],
            device_id={"sp": other}, device_id_type=MESH,
        )

    loads[3].wait()
    wo_copy(0, x, 0, wo_half, xs[1]).start()
    wo_copy(1, x, 0, wo_half, xs[3]).start()

    def wo_middle():
        quarter = wo_half // 2
        wo_copy(0, xs[3], 0, wo_half, xs[1]).wait_recv()
        wo_copy(2, xs[3], 0, quarter, xs[1]).start()
        wo_over(4, xs[3], core).start()
        wo_copy(1, xs[1], 0, wo_half, xs[3]).wait_recv()
        wo_copy(3, xs[1], quarter, quarter, xs[3]).start()
        wo_over(5, xs[1], core).start()

    def wo_end():
        quarter = wo_half // 2
        wo_copy(2, xs[2], 0, quarter, xs[1]).wait_recv()
        wo_copy(3, xs[2], quarter, quarter, xs[3]).wait_recv()
        wo_over(6, xs[2], core).start()

    def wo_wait():
        for ident, slot in ((4, xs[3]), (5, xs[1]), (6, xs[2])):
            wo_over(ident, slot, 1 - core).wait_recv()

    loads[2].wait()

    scale = 1.0 / math.sqrt(128.0) / math.log(2.0)

    def block(chip, masked):
        for j in range(4):
            h = j // 2
            kj = kbuf[pl.ds(chip * 2, 2), :, 128 * j : 128 * j + 128].reshape(2 * rows, 128)
            vj = vbuf[pl.ds(chip * 2, 2), :, 256 * h : 256 * h + 256].reshape(2 * rows, 256)
            s = lax.dot_general(
                q[:, 128 * j : 128 * j + 128], kj, (((1,), (1,)), ((), ())), preferred_element_type=F32
            )
            s = s * scale
            if masked:
                q_pos = lax.broadcasted_iota(jnp.int32, s.shape, 0) + core * rows
                s = jnp.where(lax.broadcasted_iota(jnp.int32, s.shape, 1) <= q_pos, s, -1e30)
            top = jnp.max(s, axis=1, keepdims=True)
            if masked:
                m_new = top
            else:
                m_old = m_s[j][:, :1]
                m_new = jnp.maximum(m_old, top)
                alpha = jnp.exp2(m_old - m_new)
            p = jnp.exp2(s - m_new)
            part_sum = p[:, :128]
            for i in range(1, 2 * rows // 128):
                part_sum = part_sum + p[:, 128 * i : 128 * i + 128]
            pv = jnp.dot(p.astype(BF16), vj, preferred_element_type=F32)
            m_s[j] = jnp.broadcast_to(m_new, (rows, 128))
            if masked:
                l_s[j] = part_sum
                acc[j] = pv
            else:
                l_s[j] = l_s[j] * alpha + part_sum
                acc[j] = acc[j] * alpha + pv

    keys.from_other(0, at.chip)
    vals.from_other(0, at.chip)
    block(at.chip, True)

    def first_handler():
        keys.got_first()
        vals.got_first()
        keys.got_second(0)
        vals.got_second(0)

    def second_handler():
        keys.got_opposite()
        vals.got_opposite()
        for j in (1, 2):
            keys.got_second(j)
            vals.got_second(j)

    def third_handler():
        keys.got_far(0)
        vals.got_far(0)
        wo_middle()

    def fourth_handler():
        keys.got_second(3)
        vals.got_second(3)
        loads[4].wait()
        gate.start()
        loads[5].wait()
        up.start()
        for j in (1, 2):
            keys.got_far(j)
            vals.got_far(j)

    def fifth_handler():
        keys.got_far(3)
        vals.got_far(3)

    def step(t, carry):
        for when, handler in (
            (1, first_handler), (5, second_handler), (9, third_handler), (11, fourth_handler), (15, fifth_handler)
        ):
            pl.when(t == when)(handler)
        dy, dz = (pick(t, [d[i] for d in ORDER]) for i in (0, 1))
        chip = at.chip_behind(dy, dz)
        keys.from_other(t, chip)
        vals.from_other(t, chip)

        @pl.when(chip < at.chip)
        def _():
            block(chip, False)

        return carry

    lax.fori_loop(1, 16, step, 0)

    for h in range(2):
        mixed = []
        for c in range(2):
            j = 2 * h + c
            mixed.append(acc[j] / jnp.sum(l_s[j], axis=1, keepdims=True))
        a = mixed[0] - lam[h] * mixed[1]
        square = jnp.mean(a * a, axis=1, keepdims=True)
        n = a * lax.rsqrt(square + EPS) * sub_gain[...] * (1.0 - LAMBDA_INIT)
        n_loc[:, 256 * h : 256 * h + 256] = n.astype(BF16)

    def n_copy(d, slot, to):
        return pltpu.make_async_remote_copy(
            src_ref=n_loc.at[pl.ds(to * own, own)], dst_ref=n_all.at[slot],
            send_sem=xsend.at[6 + d], recv_sem=xrecv.at[6 + d], device_id={"tp": to}, device_id_type=MESH,
        )

    for d in range(1, 4):
        n_copy(d, x, xs[d]).start()
    n_all[pl.ds(x, 1)] = n_loc[pl.ds(pl.multiple_of(x * own, own), own), :].reshape(1, own, n_loc.shape[1])
    wo_end()
    gate.got_first()
    up.got_first()
    for d in range(1, 4):
        n_copy(d, xs[4 - d], xs[d]).wait_recv()
    wo_wait()
    loads[7].wait()

    def project(i, carry):
        cols = pl.ds(pl.multiple_of(i * 256, 256), 256)
        total = res[:, cols].astype(F32)
        for j in range(4):
            total = total + jnp.dot(n_all[j], wo[j, :, cols], preferred_element_type=F32)
        mid[:, cols] = total
        return carry

    lax.fori_loop(0, mid.shape[1] // 256, project, 0)
    middle = mid[...]
    square = jnp.mean(middle * middle, axis=1, keepdims=True)
    mine = (middle * lax.rsqrt(square + EPS) * norm_gain[...]).astype(BF16)
    hn[pl.ds(x, 1)] = mine.reshape(1, *mine.shape)

    def hn_copy(ident, slot, start, size, to):
        ref = hn.at[slot, pl.ds(start, size)]
        return pltpu.make_async_remote_copy(
            src_ref=ref, dst_ref=ref, send_sem=xsend.at[10 + ident], recv_sem=xrecv.at[10 + ident],
            device_id={"tp": to}, device_id_type=MESH,
        )

    hn_copy(0, x, 0, own, xs[1]).start()
    hn_copy(1, x, 0, own, xs[3]).start()
    gate.got_second(0)
    up.got_second(0)
    gate.got_opposite()
    up.got_opposite()
    hn_copy(0, xs[3], 0, own, xs[1]).wait_recv()
    hn_copy(2, xs[3], 0, own // 2, xs[1]).start()
    hn_copy(1, xs[1], 0, own, xs[3]).wait_recv()
    hn_copy(3, xs[1], own // 2, own // 2, xs[3]).start()
    for j in (1, 2):
        gate.got_second(j)
        up.got_second(j)
    gate.got_far(0)
    up.got_far(0)
    gate.got_second(3)
    up.got_second(3)
    hn_copy(2, xs[2], 0, own // 2, xs[1]).wait_recv()
    hn_copy(3, xs[2], own // 2, own // 2, xs[3]).wait_recv()
    for j in (1, 2, 3):
        gate.got_far(j)
        up.got_far(j)
    for t in range(16):
        chip = at.chip_behind(*ORDER[t])
        gate.from_other(t, chip)
        up.from_other(t, chip)
    loads[6].wait()

    feats = hn.shape[2]
    hidden_units = wg.shape[2]

    def mix(g, taps):
        return taps[0:1] * pltpu.roll(g, 2, 0) + taps[1:2] * pltpu.roll(g, 1, 0) + taps[2:3] * g

    def gated(gc, uc):
        return (gc * (1.0 / (1.0 + jnp.exp(-gc))) * uc).astype(BF16)

    def feed(at_col, width):
        cols = pl.ds(at_col, width)
        normed = hn[...].reshape(rows, feats)
        mixed = []
        for i, (w, taps) in enumerate(((wg, conv_g), (wu, conv_u))):
            pre = jnp.dot(normed, w[:, :, cols].reshape(feats, width), preferred_element_type=F32).astype(BF16)
            tail[i, :, cols] = pre[rows - 16 :]
            head[i, :, cols] = pre[:16]
            mixed.append(mix(pre.astype(F32), taps[:, cols]))
        hid[:, cols] = gated(*mixed)

    def feed_step(i, carry):
        feed(pl.multiple_of(i * 256, 256), 256)
        return carry

    whole = hidden_units // 256
    lax.fori_loop(0, whole, feed_step, 0)
    if hidden_units % 256:
        feed(whole * 256, hidden_units % 256)

    def halo_copy(to):
        return pltpu.make_async_remote_copy(
            src_ref=tail, dst_ref=halo, send_sem=xsend.at[14], recv_sem=xrecv.at[14],
            device_id={"sp": to}, device_id_type=MESH,
        )

    halo_copy(after).start()

    def part_copy(i, slot, to):
        cols = pl.ds(pl.multiple_of(i * 512, 512), 512)
        return pltpu.make_async_remote_copy(
            src_ref=part.at[pl.ds(to * own, own), cols], dst_ref=parts.at[slot, :, cols],
            send_sem=psend.at[to, i], recv_sem=precv.at[slot, i], device_id={"tp": to}, device_id_type=MESH,
        )

    def lower(first, last):
        def body(i, carry):
            cols = pl.ds(pl.multiple_of(i * 512, 512), 512)
            part[first * own : last * own, cols] = jnp.dot(
                hid[first * own : last * own, :], wd[:, cols], preferred_element_type=F32
            ).astype(BF16)
            for to in range(first, last):
                @pl.when(x != to)
                def _():
                    part_copy(i, x, to).start()
            return carry

        lax.fori_loop(0, part.shape[1] // 512, body, 0)

    lower(1, 4)
    halo_copy(before).wait_recv()
    mixed = []
    for i, taps in enumerate((conv_g, conv_u)):
        old = jnp.where(sp == 0, 0.0, halo[i].astype(F32))
        both = jnp.concatenate([old, head[i].astype(F32)], axis=0)
        mixed.append(mix(both, taps[...])[16:])
    hid[:16, :] = gated(*mixed)
    lower(0, 1)

    chunks = part.shape[1] // 512
    for src in range(4):
        @pl.when(x != src)
        def _():
            for i in range(chunks):
                part_copy(i, src, x).wait_recv()

        @pl.when(x == src)
        def _():
            parts[src] = part[src * own : (src + 1) * own, :]

    total = parts[0].astype(F32)
    for src in range(1, 4):
        total = total + parts[src].astype(F32)
    out[...] = (mid[...] + total).astype(BF16)

    for gather in (keys, vals, gate, up):
        gather.drain()
    quarter = wo_half // 2
    wo_copy(0, x, 0, wo_half, xs[1]).wait_send()
    wo_copy(1, x, 0, wo_half, xs[1]).wait_send()
    wo_copy(2, x, 0, quarter, xs[1]).wait_send()
    wo_copy(3, x, 0, quarter, xs[1]).wait_send()
    for ident in (4, 5, 6):
        wo_over(ident, x, core).wait_send()
    for d in range(1, 4):
        n_copy(d, x, xs[d]).wait_send()
    hn_copy(0, x, 0, own, xs[1]).wait_send()
    hn_copy(1, x, 0, own, xs[1]).wait_send()
    hn_copy(2, x, 0, own // 2, xs[1]).wait_send()
    hn_copy(3, x, 0, own // 2, xs[1]).wait_send()
    halo_copy(after).wait_send()
    for to in range(4):
        @pl.when(x != to)
        def _():
            for i in range(chunks):
                part_copy(i, x, to).wait_send()


def local(
    residual, queries, key_rows, values, lambda_head, sub_gain, w_out, norm_gain, w_gate, w_up, conv_gate, conv_up,
    w_down,
):
    rows = queries.shape[0]
    d = residual.shape[1]
    own = rows // 4
    heads_wide = queries.shape[1] * values.shape[2]
    units = w_gate.shape[1]
    maps = queries.shape[1] * 2
    places = 32
    hbm = pl.BlockSpec(memory_space=pl.ANY)
    vmem = pl.BlockSpec(memory_space=pltpu.VMEM)
    smem = pl.BlockSpec(memory_space=pltpu.SMEM)
    dma = pltpu.SemaphoreType.DMA
    call = pl.pallas_call(
        kernel,
        out_shape=jax.ShapeDtypeStruct((own, d), BF16),
        in_specs=[smem] + [vmem] * 4 + [hbm] * 8,
        out_specs=vmem,
        scratch_shapes=[
            pltpu.VMEM((rows, 512), BF16),
            pltpu.VMEM((places, rows, 512), BF16),
            pltpu.VMEM((places, rows, 512), BF16),
            pltpu.VMEM((places, w_gate.shape[0], units), BF16),
            pltpu.VMEM((places, w_gate.shape[0], units), BF16),
            pltpu.VMEM((4, *w_out.shape), BF16),
            pltpu.VMEM(w_down.shape, BF16),
            pltpu.VMEM((own, d), BF16),
            pltpu.VMEM((maps, rows, 128), F32),
            pltpu.VMEM((maps, rows, 128), F32),
            pltpu.VMEM((maps, rows, values.shape[2]), F32),
            pltpu.VMEM((rows, heads_wide), BF16),
            pltpu.VMEM((4, own, heads_wide), BF16),
            pltpu.VMEM((own, d), F32),
            pltpu.VMEM((4, own, d), BF16),
            pltpu.VMEM((rows, units), BF16),
            pltpu.VMEM((2, 16, units), BF16),
            pltpu.VMEM((2, 16, units), BF16),
            pltpu.VMEM((2, 16, units), BF16),
            pltpu.VMEM((rows, d), BF16),
            pltpu.VMEM((4, own, d), BF16),
            dma((8,)), dma((80,)), dma((80,)), dma((4, 16)), dma((4, 16)), dma((16,)), dma((16,)),
            dma((4, d // 512)), dma((4, d // 512)),
        ],
        compiler_params=pltpu.CompilerParams(
            collective_id=0, has_side_effects=True, vmem_limit_bytes=67043328
        ),
    )
    return call(
        lambda_head, sub_gain[None], norm_gain[None], conv_gate, conv_up,
        queries.reshape(rows, 512), key_rows.reshape(rows, 512), values.reshape(rows, 512),
        w_gate, w_up, w_out, w_down, residual,
    )


def solution(mesh):
    placed = (
        P("sp", None),
        P("sp", "tp", None, None),
        P("sp", "tp", None, None),
        P("sp", "tp", None),
        P("tp"),
        P(),
        P("tp", None),
        P(),
        P("sp", "tp"),
        P("sp", "tp"),
        P(None, "tp"),
        P(None, "tp"),
        P("tp", None),
    )
    return jax.shard_map(
        local, mesh=mesh, in_specs=placed, out_specs=P(("sp", "tp"), None), check_vma=False
    )
```

time: 244 us -> 120 us (0.49)
  Pallas kernels: 0 us -> 112 us
  waiting for transfers between devices: 110 us -> 0 us
  matrix products: 49.1 us -> 0 us
  other arithmetic: 26 us -> 0 us
  blocking collectives: 17.3 us -> 0 us
  starting transfers between devices: 15.9 us -> 0 us
  between operations: 13.7 us -> 0.01 us
  local copies, waits for them, and re-layouts: 11.3 us -> 6.84 us
    pallas_call x0 -> x1, Pallas kernels: none -> 112 us  [local(): call(lambda_head, sub_gain[None], norm_gain[None], conv_gate, conv_up, qu...]
    all_gather x2 -> x0, waiting for transfers between devices: 80.2 us -> none  [the longest x1 80.2 us: side_by_side(): filled, at, done = (lax.all_gather(both, axis, axis=dim, tiled=True), 0, [])]
    dot_general x6 -> x0, matrix products: 49.1 us -> none  [the longest x1 18.3 us: local(): jnp.einsum('hcqk,khe->hcqe', weights.astype(jnp.bfloat16), val_part, pref...]
    all_to_all x2 -> x0, waiting for transfers between devices: 28.6 us -> none  [the longest x1 14.9 us: sum_at_owner(): lax.all_to_all(blocks, axis, split_axis=0, concat_axis=0, tiled=True)]
    reduce_sum x5 -> x0, other arithmetic: 18.5 us -> none  [the longest x1 15.7 us: local(): run_sum = jnp.sum(weights, axis=-1)]
    all_to_all x1 -> x0, blocking collectives: 17.3 us -> none  [sum_at_owner(): lax.all_to_all(blocks, axis, split_axis=0, concat_axis=0, tiled=True)]
    all_to_all x2 -> x0, starting transfers between devices: 8.78 us -> none  [the longest x1 4.41 us: copy_for_each(): lax.all_to_all(jnp.broadcast_to(array[None], (devices, *array.shape)), ax...]
    slice x4 -> x0, local copies, waits for them, and re-layouts: 7.73 us -> none  [the longest x1 7.62 us: side_by_side(): share = filled[..., at:at + column.shape[along]]]
  transfers between devices with their start and end apart: 6 -> 0, of which waited for: 4 -> 0; matrix products, arithmetic and copies ran while one was open for 30% -> 0% of each run, Pallas kernels for 0% -> 0%
where the time goes in v1:
time: 120 us; the launch traced here: 119 us
  Pallas kernels  112 us (93%)
  local copies, waits for them, and re-layouts  6.84 us (6%)
    pallas_call x1, Pallas kernels, local(): call(lambda_head, sub_gain[None], norm_gain[None], conv_gate, conv_up, qu...  112 us
    unnamed x2, local copies, waits for them, and re-layouts  3.35 us

profile of v1, /device:TPU:1, one launch (start us, length us, event | category | flops | bytes accessed | tf_op | source)
XLA Modules:
  0.0 118.9 jit_solution(11038250189391023752)
XLA Ops:
  0.0 1.8 %reshape.9.q_in = bf16[256,512]{1,0:T(8,128)(2,1)} reshape(bf16[256,2,2,128]{3,2,1,0:T(2,128)(2,1)} %param.14) | data formatting | bytes 524288 | tf_op jit(solution)/shard_map/reshape | solution.py:550
  1.8 1.7 %reshape.10.k_in = bf16[256,512]{1,0:T(8,128)(2,1)} reshape(bf16[256,2,2,128]{3,2,1,0:T(2,128)(2,1)} %param.15) | data formatting | bytes 524288 | tf_op jit(solution)/shard_map/reshape | solution.py:550
  3.5 1.7 %copy.14 = bf16[32,8,2,256]{3,1,2,0:T(8,128)(2,1)} copy(bf16[32,8,2,256]{3,2,1,0:T(2,128)(2,1)} %bitcast.5) | data formatting | bytes 524288
  5.2 112.1 %shard_map.127 = bf16[64,2048]{1,0:T(8,128)(2,1)} custom-call(f32[2]{0:T(128)} %lam.1, f32[1,256]{1,0:T(1,128)} %bitcast.7, f32[1,2048]{1,0:T(1,128)} %bitcast.6, f32[3,1408]{1,0:T(4,128)} %conv_g.1, f32[3,1408]{1,0:T(4,128)} %conv_u.1, bf16[256,512]{1,0:T(8,128)(2,1)} %reshape.9.q_in, bf16[256,512]{1,0:T(8,128)(2,1)} %reshape.10.k_in, ...), custom_call_target="tpu_custom_call" | custom-call | tf_op jit(solution)/shard_map/pallas_call | solution.py:548
  117.3 1.7 %copy.16 = bf16[64,2048]{1,0:T(8,128)(2,1)} copy(bf16[64,2048]{1,0:T(8,128)(2,1)} %shard_map.127) | data formatting | bytes 524288

commit v2 on v1

v2 whole, which is shorter than its diff:
```python
import functools
import math

import jax
import jax.numpy as jnp
from jax import lax
from jax.experimental import pallas as pl
from jax.experimental.pallas import tpu as pltpu
from jax.sharding import PartitionSpec as P

EPS = 1e-06
LAMBDA_INIT = 0.8 - 0.6 * math.exp(-0.3)
BF16, F32 = jnp.bfloat16, jnp.float32
MESH = pl.DeviceIdType.MESH

ORDER = (
    (0, 0),
    (1, 0), (3, 0), (0, 1), (0, 3),
    (1, 1), (1, 3), (3, 1), (3, 3),
    (2, 0), (0, 2),
    (2, 1), (2, 3), (1, 2), (3, 2),
    (2, 2),
)
STEP_OF = {d: t for t, d in enumerate(ORDER)}
FIRST = (0, 1, 3, 2)
HALF_ORDER = ((0, 0), (1, 0), (3, 0), (0, 1), (2, 0), (1, 1), (3, 1), (2, 1))
HALF_STEP_OF = {d: t for t, d in enumerate(HALF_ORDER)}


def pick(t, values):
    return sum(jnp.where(t == i, v, 0) for i, v in enumerate(values) if v)


def remote(src, dst, send, recv, **to):
    return pltpu.make_async_remote_copy(
        src_ref=src, dst_ref=dst, send_sem=send, recv_sem=recv, device_id=to, device_id_type=MESH
    )


class Where:
    def __init__(self):
        self.sp = lax.axis_index("sp")
        self.x = lax.axis_index("tp")
        self.core = lax.rem(self.sp, 2)
        self.other = self.sp + 1 - 2 * self.core
        self.chip = self.sp // 2
        self.y = lax.rem(self.chip, 4)
        self.z = self.chip // 4
        self.zl = lax.rem(self.z, 2)
        self.late = self.z // 2

    def chip_behind(self, dy, dz):
        return lax.rem(self.z + 4 - dz, 4) * 4 + lax.rem(self.y + 4 - dy, 4)

    def step(self, axis, forward):
        d = 3 if forward else 1
        return (self.chip_behind(d, 0) if axis == "y" else self.chip_behind(0, d)) * 2 + self.core

    def pair(self):
        return ((self.z + 1 - 2 * self.zl) * 4 + self.y) * 2 + self.core

    def opposite(self):
        return ((3 - self.z) * 4 + self.y) * 2 + self.core

    def half_chip(self, dy, zo):
        zl = self.zl + zo - 2 * zo * self.zl
        return zl * 4 + lax.rem(self.y + 4 - dy, 4)


class Gather:
    def __init__(self, at, buf, first, send, recv, drecv):
        self.at, self.buf, self.send, self.recv, self.drecv = at, buf, send, recv, drecv
        self.axes = {"f": first, "g": "z" if first == "y" else "y"}
        self.half = buf.shape[1] // 2

    def slot(self, df, dg):
        dy, dz = (df, dg) if self.axes["f"] == "y" else (dg, df)
        return self.at.chip_behind(dy, dz) * 2 + self.at.core

    def copy(self, ident, slot, half, to):
        ref = self.buf.at[slot]
        if half is not None:
            ref = self.buf.at[slot, pl.ds(half * self.half, self.half)]
        return remote(ref, ref, self.send, self.recv.at[ident], sp=to)

    def out(self, ident, df, dg, half, axis, forward):
        self.copy(ident, self.slot(df, dg), half, self.at.step(self.axes[axis], forward)).start()

    def into(self, ident, df, dg):
        self.copy(ident, self.slot(df, dg), None, self.at.other).wait_recv()

    def across(self, df, dg):
        ref = self.buf.at[self.slot(df, dg)]
        remote(ref, ref, self.send, self.drecv, sp=self.at.other).start()

    def start_along(self, axis, forward):
        self.out((0 if axis == "f" else 3) + (not forward), 0, 0, None, axis, forward)

    def along_second(self, j):
        self.second_step(j, True)
        self.second_step(j, False)
        self.across(FIRST[j], 0)

    def second_step(self, j, forward):
        self.out((3 if forward else 4) + 3 * j, FIRST[j], 0, None, "g", forward)

    def got_first(self):
        self.into(0, 1, 0)
        self.into(1, 3, 0)

    def first_step(self, forward):
        if forward:
            self.out(2, 1, 0, 0, "f", True)
        else:
            self.out(2, 3, 0, 1, "f", False)

    def got_second(self, j):
        self.into(3 + 3 * j, FIRST[j], 1)
        self.out(5 + 3 * j, FIRST[j], 1, 0, "g", True)
        self.into(4 + 3 * j, FIRST[j], 3)
        self.out(5 + 3 * j, FIRST[j], 3, 1, "g", False)
        self.across(FIRST[j], 1)
        self.across(FIRST[j], 3)

    def got_opposite(self):
        self.into(2, 2, 0)
        self.along_second(3)

    def got_far(self, j):
        self.into(5 + 3 * j, FIRST[j], 2)
        self.across(FIRST[j], 2)

    def from_other(self):
        ref = self.buf.at[pl.ds(0, 16)]
        remote(ref, ref, self.send, self.drecv, sp=self.at.other).wait_recv()

    def drain(self):
        ref = self.buf.at[pl.ds(0, 31)]
        remote(ref, ref, self.send, self.drecv, sp=self.at.other).wait_send()


class HalfGather:
    def __init__(self, at, buf, send, recv, drecv):
        self.at, self.buf, self.send, self.recv, self.drecv = at, buf, send, recv, drecv
        self.half = buf.shape[1] // 2

    def slot(self, dy, zo):
        return self.at.half_chip(dy, zo) * 2 + self.at.core

    def copy(self, ident, dy, zo, half, to):
        ref = self.buf.at[self.slot(dy, zo)]
        if half is not None:
            ref = self.buf.at[self.slot(dy, zo), pl.ds(half * self.half, self.half)]
        return remote(ref, ref, self.send, self.recv.at[ident], sp=to)

    def out(self, ident, dy, zo, half, to):
        self.copy(ident, dy, zo, half, to).start()

    def into(self, ident, dy, zo):
        self.copy(ident, dy, zo, None, self.at.other).wait_recv()

    def over(self, t, slot):
        ref = self.buf.at[slot]
        return remote(ref, ref, self.send, self.drecv.at[t], sp=self.at.other)

    def across(self, dy, zo):
        self.over(HALF_STEP_OF[dy, zo], self.slot(dy, zo)).start()

    def from_other(self, t, chip):
        self.over(t, chip * 2 + 1 - self.at.core).wait_recv()

    def ring_start(self, ident, zo):
        self.out(ident, 0, zo, None, self.at.step("y", True))
        self.out(ident + 1, 0, zo, None, self.at.step("y", False))

    def ring_middle(self, ident, zo, after=lambda dy: None):
        self.into(ident, 1, zo)
        self.out(ident + 2, 1, zo, 0, self.at.step("y", True))
        after(1)
        self.across(1, zo)
        self.into(ident + 1, 3, zo)
        self.out(ident + 2, 3, zo, 1, self.at.step("y", False))
        after(3)
        self.across(3, zo)

    def ring_end(self, ident, zo, after=lambda dy: None):
        self.into(ident + 2, 2, zo)
        after(2)
        self.across(2, zo)

    def drain(self):
        ref = self.buf.at[pl.ds(0, 15)]
        remote(ref, ref, self.send, self.recv.at[0], sp=self.at.other).wait_send()


def kernel(
    lam, sub_gain, norm_gain, conv_g, conv_u,
    q_in, k_in, v_in, wg_in, wu_in, wo_in, wd_in, res_in,
    out,
    q_raw, k_raw, v_raw, q, kbuf, vbuf, wg, wu, wo, wd, res,
    m_s, l_s, acc, a_far, stat, stat_far, n_loc, n_all, mid, hn, hid, part, relay, parts,
    lsem, send, krecv, kdrecv, wrecv, drecv, orecv, xrecv, precv,
):
    at = Where()
    x, sp, core, other = at.x, at.sp, at.core, at.other
    rows = q.shape[1]
    own = rows // 4
    late = at.late == 1
    early = at.late == 0
    mine = at.half_chip(0, 0)

    loads = [
        pltpu.make_async_copy(src, dst, lsem.at[i])
        for i, (src, dst) in enumerate(
            (
                (k_in, k_raw), (v_in, v_raw), (q_in, q_raw), (wo_in, wo.at[x]),
                (wg_in, wg.at[sp]), (wu_in, wu.at[sp]), (wd_in, wd), (res_in.at[pl.ds(x * own, own)], res),
            )
        )
    ]
    for load in loads:
        load.start()

    barrier = pltpu.get_barrier_semaphore()
    after, before = lax.rem(sp + 1, 32), lax.rem(sp + 31, 32)
    for to in (
        other, at.step("y", True), at.step("y", False), at.step("z", True), at.step("z", False), after, before
    ):
        pl.semaphore_signal(barrier, inc=1, device_id={"sp": to}, device_id_type=MESH)
    xs = [lax.rem(x + d, 4) for d in range(4)]
    for to in xs[1:]:
        pl.semaphore_signal(barrier, inc=1, device_id={"tp": to}, device_id_type=MESH)
    for load, raw, laid in (
        (loads[0], k_raw, kbuf.at[mine * 2 + core]), (loads[1], v_raw, vbuf.at[mine * 2 + core]), (loads[2], q_raw, q.at[0])
    ):
        load.wait()
        laid[...] = raw[...].reshape(laid.shape)
    with jax.named_scope("barrier"):
        pl.semaphore_wait(barrier, 10)

    keys = HalfGather(at, kbuf, send.at[0], krecv.at[0], kdrecv.at[0])
    vals = HalfGather(at, vbuf, send.at[1], krecv.at[1], kdrecv.at[1])
    gate = Gather(at, wg, "y", send.at[2], wrecv.at[0], drecv.at[0])
    up = Gather(at, wu, "z", send.at[3], wrecv.at[1], drecv.at[1])

    def key_on(dy):
        keys.out(3 + FIRST.index(dy), dy, 0, None, at.pair())

    def q_copy():
        return remote(q.at[0], q.at[1], send.at[9], orecv.at[0], sp=at.opposite())

    keys.ring_start(0, 0)
    vals.out(0, 0, 0, None, at.pair())
    key_on(0)
    vals.ring_start(1, 0)
    keys.across(0, 0)
    vals.across(0, 0)

    @pl.when(late)
    def _():
        q_copy().start()

    def weights_along_z(forward):
        gate.start_along("g", forward)
        up.start_along("f", forward)

    loads[4].wait()
    loads[5].wait()
    for forward in (True, False):
        pl.when(at.zl == int(forward))(functools.partial(weights_along_z, forward))

    def weights_start():
        for forward in (True, False):
            gate.start_along("f", forward)
            up.start_along("g", forward)
            pl.when(at.zl == int(not forward))(functools.partial(weights_along_z, forward))
        gate.across(0, 0)
        up.across(0, 0)

    wo_half = wo.shape[1] // 2
    wo_quarter = wo_half // 2

    def wo_copy(ident, slot, start, size, to):
        ref = wo.at[slot, pl.ds(core * wo_half + start, size)]
        return remote(ref, ref, send.at[4], xrecv.at[ident], tp=to)

    def wo_over(slot):
        ref = wo.at[slot, pl.ds(core * wo_half, wo_half)]
        return remote(ref, ref, send.at[4], xrecv.at[3], sp=other)

    loads[3].wait()
    wo_copy(0, x, 0, wo_half, xs[1]).start()
    wo_copy(1, x, 0, wo_half, xs[3]).start()

    def wo_middle():
        wo_copy(0, xs[3], 0, wo_half, xs[1]).wait_recv()
        wo_copy(2, xs[3], 0, wo_quarter, xs[1]).start()
        wo_over(xs[3]).start()
        wo_copy(1, xs[1], 0, wo_half, xs[3]).wait_recv()
        wo_copy(2, xs[1], wo_quarter, wo_quarter, xs[3]).start()
        wo_over(xs[1]).start()

    def wo_end():
        wo_copy(2, xs[2], 0, wo_half, xs[1]).wait_recv()
        wo_over(xs[2]).start()

    def wo_wait():
        ref = wo.at[pl.ds(0, 3), pl.ds(0, wo_half)]
        remote(ref, ref, send.at[4], xrecv.at[3], sp=other).wait_recv()

    scale = 1.0 / math.sqrt(128.0) / math.log(2.0)

    def block(who, chip, masked):
        for j in range(4):
            h = j // 2
            kj = kbuf[pl.ds(chip * 2, 2), :, 128 * j : 128 * j + 128].reshape(2 * rows, 128)
            vj = vbuf[pl.ds(chip * 2, 2), :, 256 * h : 256 * h + 256].reshape(2 * rows, 256)
            s = lax.dot_general(
                q[who, :, 128 * j : 128 * j + 128], kj, (((1,), (1,)), ((), ())), preferred_element_type=F32
            )
            s = s * scale
            if masked:
                q_pos = lax.broadcasted_iota(jnp.int32, s.shape, 0) + core * rows
                s = jnp.where(lax.broadcasted_iota(jnp.int32, s.shape, 1) <= q_pos, s, -1e30)
            top = jnp.max(s, axis=1, keepdims=True)
            if masked:
                m_new = top
            else:
                m_old = m_s[4 * who + j][:, :1]
                m_new = jnp.maximum(m_old, top)
                alpha = jnp.exp2(m_old - m_new)
            p = jnp.exp2(s - m_new)
            part_sum = p[:, :128]
            for i in range(1, 2 * rows // 128):
                part_sum = part_sum + p[:, 128 * i : 128 * i + 128]
            pv = jnp.dot(p.astype(BF16), vj, preferred_element_type=F32)
            m_s[4 * who + j] = jnp.broadcast_to(m_new, (rows, 128))
            if masked:
                l_s[4 * who + j] = part_sum
                acc[4 * who + j] = pv
            else:
                l_s[4 * who + j] = l_s[4 * who + j] * alpha + part_sum
                acc[4 * who + j] = acc[4 * who + j] * alpha + pv

    @pl.when(early)
    def _():
        m_s[4:] = jnp.full((4, rows, 128), -1e30, F32)
        l_s[4:] = jnp.zeros((4, rows, 128), F32)
        acc[4:] = jnp.zeros((4, *acc.shape[1:]), F32)

    with jax.named_scope("own_wait"):
        keys.from_other(0, mine)
        vals.from_other(0, mine)
    with jax.named_scope("own_block"):
        block(0, mine, True)

    def handler_0():
        keys.ring_middle(0, 0, key_on)
        vals.into(0, 0, 1)
        vals.ring_start(4, 1)
        vals.across(0, 1)
        vals.ring_middle(1, 0)
        keys.into(3, 0, 1)
        keys.across(0, 1)

        @pl.when(early)
        def _():
            q_copy().wait_recv()

    def handler_2():
        keys.ring_end(0, 0, key_on)

    def handler_4():
        vals.ring_middle(4, 1)
        weights_start()
        vals.ring_end(1, 0)

    def handler_5():
        keys.into(4, 1, 1)
        keys.across(1, 1)
        keys.into(5, 3, 1)
        keys.across(3, 1)

    def handler_7():
        vals.ring_end(4, 1)
        keys.into(6, 2, 1)
        keys.across(2, 1)
        wo_middle()

    def step(t, carry):
        for when, handler in (
            (0, handler_0), (2, handler_2), (4, handler_4), (5, handler_5), (7, handler_7)
        ):

            @pl.when(t == when)
            def _():
                with jax.named_scope(handler.__name__):
                    handler()

        dy, zo = (pick(t, [d[i] for d in HALF_ORDER]) for i in (0, 1))
        chip = at.half_chip(dy, zo)

        @pl.when(t > 0)
        def _():
            with jax.named_scope("d2d_wait"):
                keys.from_other(t, chip)
                vals.from_other(t, chip)

        @pl.when(early)
        def _():
            with jax.named_scope("far_block"):
                block(1, chip, False)

        @pl.when(chip < mine)
        def _():
            with jax.named_scope("block"):
                block(0, chip, False)

        return carry

    lax.fori_loop(0, 8, step, 0)

    def stat_copy():
        return remote(stat, stat_far, send.at[10], orecv.at[1], sp=at.opposite())

    def a_copy(h):
        return remote(a_far.at[h], a_far.at[h], send.at[11], orecv.at[2 + h], sp=at.opposite())

    lanes = lax.broadcasted_iota(jnp.int32, (rows, 128), 1)
    base = 4 - 4 * at.late
    stats = jnp.zeros((rows, 128), F32)
    for j in range(4):
        total = jnp.sum(l_s[base + j], axis=1, keepdims=True)
        stats = jnp.where(lanes == j, m_s[base + j], jnp.where(lanes == 4 + j, total, stats))
    stat[...] = stats.T[:8]
    stat_copy().start()

    def weights_on_along_z(forward):
        up.first_step(forward)
        gate.second_step(1, forward)
        gate.second_step(2, forward)

    with jax.named_scope("w_first"):
        gate.got_first()
        for forward in (True, False):
            gate.first_step(forward)
        up.got_first()
        for forward in (True, False):
            pl.when(at.zl == int(not forward))(functools.partial(weights_on_along_z, forward))
        for j in (1, 2):
            up.along_second(j)
            gate.across(FIRST[j], 0)

    with jax.named_scope("stat_wait"):
        stat_copy().wait_recv()

    with jax.named_scope("blend"):
        here = jnp.concatenate([stat[...], jnp.zeros((120, rows), F32)], axis=0).T
        there = jnp.concatenate([stat_far[...], jnp.zeros((120, rows), F32)], axis=0).T
        for h in range(2):
            shares = []
            for j in (2 * h, 2 * h + 1):
                m_here, m_there = here[:, j : j + 1], there[:, j : j + 1]
                top = jnp.maximum(m_here, m_there)
                e_here, e_there = jnp.exp2(m_here - top), jnp.exp2(m_there - top)
                total = here[:, 4 + j : 5 + j] * e_here + there[:, 4 + j : 5 + j] * e_there
                shares.append(acc[base + j] * (e_here / total))
            a = shares[0] - lam[h] * shares[1]

            @pl.when(early)
            def _():
                a_far[h] = a.astype(BF16)
                a_copy(h).start()

            @pl.when(late)
            def _():
                acc[2 * h] = a

    for forward in (True, False):
        pl.when(at.zl == int(forward))(functools.partial(weights_on_along_z, forward))

    with jax.named_scope("w_second"):
        gate.got_second(0)
        up.got_second(0)
        gate.got_opposite()
        up.got_opposite()

    for h in range(2):

        @pl.when(late)
        def _():
            with jax.named_scope("a_wait"):
                a_copy(h).wait_recv()
            acc[2 * h] = acc[2 * h] + a_far[h].astype(F32)

        @pl.when(early)
        def _():
            mixed = []
            for j in (2 * h, 2 * h + 1):
                mixed.append(acc[j] / jnp.sum(l_s[j], axis=1, keepdims=True))
            acc[2 * h] = mixed[0] - lam[h] * mixed[1]

        a = acc[2 * h]
        square = jnp.mean(a * a, axis=1, keepdims=True)
        n = a * lax.rsqrt(square + EPS) * sub_gain[...] * (1.0 - LAMBDA_INIT)
        n_loc[:, 256 * h : 256 * h + 256] = n.astype(BF16)

    def n_copy(d, slot, to):
        return remote(n_loc.at[pl.ds(to * own, own)], n_all.at[slot], send.at[5], xrecv.at[4 + d], tp=to)

    for d in range(1, 4):
        n_copy(d, x, xs[d]).start()
    n_all[pl.ds(x, 1)] = n_loc[pl.ds(pl.multiple_of(x * own, own), own), :].reshape(1, own, n_loc.shape[1])
    with jax.named_scope("wo_end"):
        wo_end()
    with jax.named_scope("w_third"):
        for j in (1, 2):
            gate.got_second(j)
            up.got_second(j)
    with jax.named_scope("n_wait"):
        for d in range(1, 4):
            n_copy(d, xs[4 - d], xs[d]).wait_recv()
    with jax.named_scope("wo_wait"):
        wo_wait()
        loads[7].wait()

    def project(i, carry):
        cols = pl.ds(pl.multiple_of(i * 256, 256), 256)
        total = res[:, cols].astype(F32)
        for j in range(4):
            total = total + jnp.dot(n_all[j], wo[j, :, cols], preferred_element_type=F32)
        mid[:, cols] = total
        return carry

    with jax.named_scope("project"):
        lax.fori_loop(0, mid.shape[1] // 256, project, 0, unroll=True)
    middle = mid[...]
    square = jnp.mean(middle * middle, axis=1, keepdims=True)

    def hn_at(slot, start, size):
        return pl.ds(pl.multiple_of(16 + slot * own + start, 16), size)

    hn[hn_at(x, 0, own), :] = (middle * lax.rsqrt(square + EPS) * norm_gain[...]).astype(BF16)

    def hn_copy(ident, slot, start, size, to):
        ref = hn.at[hn_at(slot, start, size)]
        return remote(ref, ref, send.at[6], xrecv.at[8 + ident], tp=to)

    def halo_copy(to):
        return remote(hn.at[pl.ds(rows, 16)], hn.at[pl.ds(0, 16)], send.at[7], xrecv.at[11], sp=to)

    hn_copy(0, x, 0, own, xs[1]).start()
    hn_copy(1, x, 0, own, xs[3]).start()
    with jax.named_scope("w_fourth"):
        gate.got_second(3)
        up.got_second(3)
    with jax.named_scope("hn_middle"):
        hn_copy(0, xs[3], 0, own, xs[1]).wait_recv()
        hn_copy(2, xs[3], 0, own // 2, xs[1]).start()
        hn_copy(1, xs[1], 0, own, xs[3]).wait_recv()
        hn_copy(2, xs[1], own // 2, own // 2, xs[3]).start()
    with jax.named_scope("w_fifth"):
        for j in range(4):
            gate.got_far(j)
            up.got_far(j)
    with jax.named_scope("hn_wait"):
        hn_copy(2, xs[2], 0, own, xs[1]).wait_recv()
    pl.when(sp < 31)(lambda: halo_copy(after).start())
    with jax.named_scope("w_over"):
        gate.from_other()
        up.from_other()
        loads[6].wait()

    @pl.when(sp > 0)
    def _():
        with jax.named_scope("halo_wait"):
            halo_copy(before).wait_recv()

    @pl.when(sp == 0)
    def _():
        hn[:16, :] = jnp.zeros((16, hn.shape[1]), BF16)


    feats = hn.shape[1]
    units = wg.shape[2]

    def mix(g, taps):
        return taps[0:1] * pltpu.roll(g, 2, 0) + taps[1:2] * pltpu.roll(g, 1, 0) + taps[2:3] * g

    def feed(at_col, width):
        cols = pl.ds(at_col, width)
        mixed = []
        for w, taps in ((wg, conv_g), (wu, conv_u)):
            pre = jnp.dot(hn[...], w[:, :, cols].reshape(feats, width), preferred_element_type=F32)
            mixed.append(mix(pre.astype(BF16).astype(F32), taps[:, cols])[16:])
        gc, uc = mixed
        hid[:, cols] = (gc * (1.0 / (1.0 + jnp.exp(-gc))) * uc).astype(BF16)

    def feed_step(i, carry):
        feed(pl.multiple_of(i * 256, 256), 256)
        return carry

    whole = units // 256
    with jax.named_scope("feed"):
        lax.fori_loop(0, whole, feed_step, 0, unroll=True)
        if units % 256:
            feed(whole * 256, units % 256)

    chunks = part.shape[2] // 512
    side = own // 2

    def cols_of(i):
        return pl.ds(pl.multiple_of(i * 512, 512), 512)

    def relay_copy(s, i, to):
        return remote(
            part.at[xs[2], pl.ds(s * side, side), cols_of(i)], relay.at[s, :, cols_of(i)],
            send.at[8], precv.at[0, s, i], tp=to,
        )

    def part_copy(s, i, to):
        return remote(
            part.at[to, :, cols_of(i)], parts.at[s, :, cols_of(i)], send.at[8], precv.at[1, s, i], tp=to
        )

    def lower(i, carry):
        cols = cols_of(i)
        full = jnp.dot(hid[...], wd[:, cols], preferred_element_type=F32).astype(BF16)
        part[:, :, cols] = full.reshape(4, own, 512)
        relay_copy(0, i, xs[1]).start()
        relay_copy(1, i, xs[3]).start()
        return carry

    with jax.named_scope("lower"):
        lax.fori_loop(0, chunks, lower, 0, unroll=True)

    def pass_on(i, carry):
        cols = cols_of(i)
        for s, to in ((0, xs[1]), (1, xs[3])):
            relay_copy(s, i, to).wait_recv()
            half = pl.ds(s * side, side)
            total = part[to, half, cols].astype(F32) + relay[s, :, cols].astype(F32)
            part[to, half, cols] = total.astype(BF16)
            part_copy(s, i, to).start()
        return carry

    with jax.named_scope("pass_on"):
        lax.fori_loop(0, chunks, pass_on, 0)

    def finish(i, carry):
        cols = cols_of(i)
        for s, to in ((0, xs[1]), (1, xs[3])):
            part_copy(s, i, to).wait_recv()
        total = parts[0, :, cols].astype(F32) + parts[1, :, cols].astype(F32) + part[x, :, cols].astype(F32)
        out[:, cols] = (mid[:, cols] + total).astype(BF16)
        return carry

    with jax.named_scope("finish"):
        lax.fori_loop(0, chunks, finish, 0)

    def sent(ref, which):
        remote(ref, ref, send.at[which], xrecv.at[0], sp=other).wait_send()

    with jax.named_scope("drain"):
        for gather in (keys, vals, gate, up):
            gather.drain()
        sent(wo.at[pl.ds(0, 3)], 4)
        sent(n_all.at[pl.ds(0, 3)], 5)
        sent(hn.at[pl.ds(0, 3 * own)], 6)
        pl.when(sp < 31)(lambda: halo_copy(after).wait_send())
        sent(hn.at[pl.ds(0, 3 * own)], 8)
        stat_copy().wait_send()

        @pl.when(late)
        def _():
            q_copy().wait_send()

        @pl.when(early)
        def _():
            sent(a_far, 11)


def local(
    residual, queries, key_rows, values, lambda_head, sub_gain, w_out, norm_gain, w_gate, w_up, conv_gate, conv_up,
    w_down,
):
    rows = queries.shape[0]
    d = residual.shape[1]
    own = rows // 4
    heads_wide = queries.shape[1] * values.shape[2]
    units = w_gate.shape[1]
    maps = queries.shape[1] * 2
    places = 32
    hbm = pl.BlockSpec(memory_space=pl.ANY)
    vmem = pl.BlockSpec(memory_space=pltpu.VMEM)
    smem = pl.BlockSpec(memory_space=pltpu.SMEM)
    dma = pltpu.SemaphoreType.DMA
    call = pl.pallas_call(
        kernel,
        out_shape=jax.ShapeDtypeStruct((own, d), BF16),
        in_specs=[smem] + [vmem] * 4 + [hbm] * 8,
        out_specs=vmem,
        scratch_shapes=[
            pltpu.VMEM(queries.shape, BF16),
            pltpu.VMEM(key_rows.shape, BF16),
            pltpu.VMEM(values.shape, BF16),
            pltpu.VMEM((2, rows, 512), BF16),
            pltpu.VMEM((places // 2, rows, 512), BF16),
            pltpu.VMEM((places // 2, rows, 512), BF16),
            pltpu.VMEM((places, w_gate.shape[0], units), BF16),
            pltpu.VMEM((places, w_gate.shape[0], units), BF16),
            pltpu.VMEM((4, *w_out.shape), BF16),
            pltpu.VMEM(w_down.shape, BF16),
            pltpu.VMEM((own, d), BF16),
            pltpu.VMEM((2 * maps, rows, 128), F32),
            pltpu.VMEM((2 * maps, rows, 128), F32),
            pltpu.VMEM((2 * maps, rows, values.shape[2]), F32),
            pltpu.VMEM((2, rows, values.shape[2]), BF16),
            pltpu.VMEM((8, rows), F32),
            pltpu.VMEM((8, rows), F32),
            pltpu.VMEM((rows, heads_wide), BF16),
            pltpu.VMEM((4, own, heads_wide), BF16),
            pltpu.VMEM((own, d), F32),
            pltpu.VMEM((rows + 16, d), BF16),
            pltpu.VMEM((rows, units), BF16),
            pltpu.VMEM((4, own, d), BF16),
            pltpu.VMEM((2, own // 2, d), BF16),
            pltpu.VMEM((2, own, d), BF16),
            dma((8,)), dma((12,)), dma((2, 7)), dma((2, 8)), dma((2, 15)), dma((2,)), dma((4,)), dma((12,)),
            dma((2, 2, d // 512)),
        ],
        compiler_params=pltpu.CompilerParams(
            collective_id=0, has_side_effects=True, vmem_limit_bytes=67043328
        ),
    )
    return call(
        lambda_head, sub_gain[None], norm_gain[None], conv_gate, conv_up,
        queries, key_rows, values,
        w_gate, w_up, w_out, w_down, residual,
    )


def solution(mesh):
    placed = (
        P("sp", None),
        P("sp", "tp", None, None),
        P("sp", "tp", None, None),
        P("sp", "tp", None),
        P("tp"),
        P(),
        P("tp", None),
        P(),
        P("sp", "tp"),
        P("sp", "tp"),
        P(None, "tp"),
        P(None, "tp"),
        P("tp", None),
    )
    return jax.shard_map(
        local, mesh=mesh, in_specs=placed, out_specs=P(("sp", "tp"), None), check_vma=False
    )
```

time: 120 us -> 99.6 us (0.83)
  the two profiles are of different devices: /device:TPU:1 before, /device:TPU:98 now
where the time goes in v2:
time: 99.6 us; the launch traced here: 99.4 us
  Pallas kernels  97.7 us (98%)
  local copies, waits for them, and re-layouts  1.67 us (2%)
    pallas_call x1, Pallas kernels, local(): call(lambda_head, sub_gain[None], norm_gain[None], conv_gate, conv_up, qu...  97.7 us

profile of v2, /device:TPU:98, one launch (start us, length us, event | category | flops | bytes accessed | tf_op | source)
XLA Modules:
  0.0 99.4 jit_solution(17051536103698859582)
XLA Ops:
  0.0 97.7 %shard_map.127 = bf16[64,2048]{1,0:T(8,128)(2,1)} custom-call(f32[2]{0:T(128)} %lam.1, f32[1,256]{1,0:T(1,128)} %bitcast.3, f32[1,2048]{1,0:T(1,128)} %bitcast.2, f32[3,1408]{1,0:T(4,128)} %conv_g.1, f32[3,1408]{1,0:T(4,128)} %conv_u.1, bf16[256,2,2,128]{3,2,1,0:T(2,128)(2,1)} %q_in.1, bf16[256,2,2,128]{3,2,1,0:T(2,128)(2,1)} %k_in.1, ...), custom_call_target="tpu_custom_call" | custom-call | tf_op jit(solution)/shard_map/pallas_call | solution.py:736
  97.7 1.7 %copy.15 = bf16[64,2048]{1,0:T(8,128)(2,1)} copy(bf16[64,2048]{1,0:T(8,128)(2,1)} %shard_map.127) | data formatting | bytes 524288

commit v3 on v2

--- a/solution.py
+++ b/solution.py
@@ -23,7 +23,7 @@
 )
 STEP_OF = {d: t for t, d in enumerate(ORDER)}
 FIRST = (0, 1, 3, 2)
-HALF_ORDER = ((0, 0), (1, 0), (3, 0), (0, 1), (2, 0), (1, 1), (3, 1), (2, 1))
+HALF_ORDER = ((0, 0), (1, 0), (3, 0), (0, 1), (1, 1), (3, 1), (2, 0), (2, 1))
 HALF_STEP_OF = {d: t for t, d in enumerate(HALF_ORDER)}
 
 
@@ -89,9 +89,9 @@
     def into(self, ident, df, dg):
         self.copy(ident, self.slot(df, dg), None, self.at.other).wait_recv()
 
-    def across(self, df, dg):
+    def across(self, df, dg, far=0):
         ref = self.buf.at[self.slot(df, dg)]
-        remote(ref, ref, self.send, self.drecv, sp=self.at.other).start()
+        remote(ref, ref, self.send, self.drecv.at[far], sp=self.at.other).start()
 
     def start_along(self, axis, forward):
         self.out((0 if axis == "f" else 3) + (not forward), 0, 0, None, axis, forward)
@@ -114,11 +114,21 @@
         else:
             self.out(2, 3, 0, 1, "f", False)
 
-    def got_second(self, j):
+    def got_second(self, j, uneven=False):
         self.into(3 + 3 * j, FIRST[j], 1)
-        self.out(5 + 3 * j, FIRST[j], 1, 0, "g", True)
         self.into(4 + 3 * j, FIRST[j], 3)
-        self.out(5 + 3 * j, FIRST[j], 3, 1, "g", False)
+
+        def pass_on(cut):
+            for df, dg, start, stop in ((FIRST[j], 1, 0, cut), (FIRST[j], 3, cut, 2 * self.half)):
+                ref = self.buf.at[self.slot(df, dg), pl.ds(start, stop - start)]
+                to = self.at.step(self.axes["g"], dg == 1)
+                remote(ref, ref, self.send, self.recv.at[5 + 3 * j], sp=to).start()
+
+        if uneven:
+            for zl, cut in ((0, self.half // 2), (1, 3 * self.half // 2)):
+                pl.when(self.at.zl == zl)(functools.partial(pass_on, cut))
+        else:
+            pass_on(self.half)
         self.across(FIRST[j], 1)
         self.across(FIRST[j], 3)
 
@@ -128,15 +138,15 @@
 
     def got_far(self, j):
         self.into(5 + 3 * j, FIRST[j], 2)
-        self.across(FIRST[j], 2)
-
-    def from_other(self):
-        ref = self.buf.at[pl.ds(0, 16)]
-        remote(ref, ref, self.send, self.drecv, sp=self.at.other).wait_recv()
+        self.across(FIRST[j], 2, 1)
+
+    def from_other(self, far):
+        ref = self.buf.at[pl.ds(0, 4 if far else 12)]
+        remote(ref, ref, self.send, self.drecv.at[far], sp=self.at.other).wait_recv()
 
     def drain(self):
         ref = self.buf.at[pl.ds(0, 31)]
-        remote(ref, ref, self.send, self.drecv, sp=self.at.other).wait_send()
+        remote(ref, ref, self.send, self.drecv.at[0], sp=self.at.other).wait_send()
 
 
 class HalfGather:
@@ -166,8 +176,9 @@
     def across(self, dy, zo):
         self.over(HALF_STEP_OF[dy, zo], self.slot(dy, zo)).start()
 
-    def from_other(self, t, chip):
-        self.over(t, chip * 2 + 1 - self.at.core).wait_recv()
+    def both_from_other(self, t):
+        ref = self.buf.at[pl.ds(0, 2)]
+        remote(ref, ref, self.send, self.drecv.at[t], sp=self.at.other).wait_recv()
 
     def ring_start(self, ident, zo):
         self.out(ident, 0, zo, None, self.at.step("y", True))
@@ -194,11 +205,11 @@
 
 
 def kernel(
-    lam, sub_gain, norm_gain, conv_g, conv_u,
+    lam_in, sub_in, norm_in, conv_g_in, conv_u_in,
     q_in, k_in, v_in, wg_in, wu_in, wo_in, wd_in, res_in,
     out,
-    q_raw, k_raw, v_raw, q, kbuf, vbuf, wg, wu, wo, wd, res,
-    m_s, l_s, acc, a_far, stat, stat_far, n_loc, n_all, mid, hn, hid, part, relay, parts,
+    lam, sub_gain, norm_gain, conv_g, conv_u, q_raw, k_raw, v_raw, q, kbuf, vbuf, wg, wu, wo, wd, res,
+    m_s, l_s, acc, a_far, stat, stat_far, n_all, mid, hn, pre, hid, part, relay, parts, ended,
     lsem, send, krecv, kdrecv, wrecv, drecv, orecv, xrecv, precv,
 ):
     at = Where()
@@ -209,37 +220,38 @@
     early = at.late == 0
     mine = at.half_chip(0, 0)
 
+    barrier = pltpu.get_barrier_semaphore()
+    after, before = lax.rem(sp + 1, 32), lax.rem(sp + 31, 32)
+    for to in (other, at.step("y", True), at.step("y", False), at.step("z", True), at.step("z", False)):
+        pl.semaphore_signal(barrier, inc=1, device_id={"sp": to}, device_id_type=MESH)
+    for to in (after, before):
+        for x_to in range(4):
+            pl.semaphore_signal(barrier, inc=1, device_id={"sp": to, "tp": x_to}, device_id_type=MESH)
+    xs = [lax.rem(x + d, 4) for d in range(4)]
+    for to in xs[1:]:
+        pl.semaphore_signal(barrier, inc=1, device_id={"tp": to}, device_id_type=MESH)
+
     loads = [
         pltpu.make_async_copy(src, dst, lsem.at[i])
         for i, (src, dst) in enumerate(
             (
-                (k_in, k_raw), (v_in, v_raw), (q_in, q_raw), (wo_in, wo.at[x]),
-                (wg_in, wg.at[sp]), (wu_in, wu.at[sp]), (wd_in, wd), (res_in.at[pl.ds(x * own, own)], res),
+                (k_in, k_raw), (v_in, v_raw), (q_in, q_raw), (wo_in, wo.at[x]), (wg_in, wg.at[sp]), (wu_in, wu.at[sp]),
+                (wd_in, wd), (res_in, res.at[pl.ds(16, rows)]), (lam_in, lam), (sub_in, sub_gain),
+                (norm_in, norm_gain), (conv_g_in, conv_g), (conv_u_in, conv_u),
             )
         )
     ]
-    for load in loads:
+    for load in loads[:3]:
         load.start()
-
-    barrier = pltpu.get_barrier_semaphore()
-    after, before = lax.rem(sp + 1, 32), lax.rem(sp + 31, 32)
-    for to in (
-        other, at.step("y", True), at.step("y", False), at.step("z", True), at.step("z", False), after, before
-    ):
-        pl.semaphore_signal(barrier, inc=1, device_id={"sp": to}, device_id_type=MESH)
-    xs = [lax.rem(x + d, 4) for d in range(4)]
-    for to in xs[1:]:
-        pl.semaphore_signal(barrier, inc=1, device_id={"tp": to}, device_id_type=MESH)
-    for load, raw, laid in (
-        (loads[0], k_raw, kbuf.at[mine * 2 + core]), (loads[1], v_raw, vbuf.at[mine * 2 + core]), (loads[2], q_raw, q.at[0])
-    ):
-        load.wait()
-        laid[...] = raw[...].reshape(laid.shape)
+    loads[0].wait()
+    kbuf[mine * 2 + core] = k_raw[...].reshape(kbuf.shape[1:])
+    for load in loads[3:6] + loads[7:]:
+        load.start()
     with jax.named_scope("barrier"):
-        pl.semaphore_wait(barrier, 10)
-
-    keys = HalfGather(at, kbuf, send.at[0], krecv.at[0], kdrecv.at[0])
-    vals = HalfGather(at, vbuf, send.at[1], krecv.at[1], kdrecv.at[1])
+        pl.semaphore_wait(barrier, 16)
+
+    keys = HalfGather(at, kbuf, send.at[0], krecv.at[0], kdrecv)
+    vals = HalfGather(at, vbuf, send.at[1], krecv.at[1], kdrecv)
     gate = Gather(at, wg, "y", send.at[2], wrecv.at[0], drecv.at[0])
     up = Gather(at, wu, "z", send.at[3], wrecv.at[1], drecv.at[1])
 
@@ -250,11 +262,15 @@
         return remote(q.at[0], q.at[1], send.at[9], orecv.at[0], sp=at.opposite())
 
     keys.ring_start(0, 0)
+    loads[1].wait()
+    vbuf[mine * 2 + core] = v_raw[...].reshape(vbuf.shape[1:])
     vals.out(0, 0, 0, None, at.pair())
     key_on(0)
     vals.ring_start(1, 0)
     keys.across(0, 0)
     vals.across(0, 0)
+    loads[2].wait()
+    q[0] = q_raw[...].reshape(q.shape[1:])
 
     @pl.when(late)
     def _():
@@ -271,7 +287,6 @@
 
     def weights_start():
         for forward in (True, False):
-            gate.start_along("f", forward)
             up.start_along("g", forward)
             pl.when(at.zl == int(not forward))(functools.partial(weights_along_z, forward))
         gate.across(0, 0)
@@ -287,6 +302,26 @@
     def wo_over(slot):
         ref = wo.at[slot, pl.ds(core * wo_half, wo_half)]
         return remote(ref, ref, send.at[4], xrecv.at[3], sp=other)
+
+    def res_copy(to):
+        return remote(res.at[pl.ds(rows, 16)], res.at[pl.ds(0, 16)], send.at[6], xrecv.at[8], sp=to)
+
+    def n_halo_copy(slot, to, x_to):
+        return remote(
+            n_all.at[slot, pl.ds(rows, 16)], n_all.at[slot, pl.ds(0, 16)], send.at[7], xrecv.at[9], sp=to, tp=x_to
+        )
+
+    loads[7].wait()
+    loads[6].start()
+
+    @pl.when(sp < 31)
+    def _():
+        res_copy(after).start()
+
+    @pl.when(sp == 0)
+    def _():
+        res[:16, :] = jnp.zeros((16, res.shape[1]), BF16)
+        n_all[:, :16, :] = jnp.zeros((4, 16, n_all.shape[2]), BF16)
 
     loads[3].wait()
     wo_copy(0, x, 0, wo_half, xs[1]).start()
@@ -349,8 +384,7 @@
         acc[4:] = jnp.zeros((4, *acc.shape[1:]), F32)
 
     with jax.named_scope("own_wait"):
-        keys.from_other(0, mine)
-        vals.from_other(0, mine)
+        keys.both_from_other(0)
     with jax.named_scope("own_block"):
         block(0, mine, True)
 
@@ -358,6 +392,8 @@
         keys.ring_middle(0, 0, key_on)
         vals.into(0, 0, 1)
         vals.ring_start(4, 1)
+        for forward in (True, False):
+            gate.start_along("f", forward)
         vals.across(0, 1)
         vals.ring_middle(1, 0)
         keys.into(3, 0, 1)
@@ -370,26 +406,32 @@
     def handler_2():
         keys.ring_end(0, 0, key_on)
 
+    def gate_along_z(forward):
+        gate.second_step(1, forward)
+        gate.second_step(2, forward)
+
     def handler_4():
         vals.ring_middle(4, 1)
+        for ident, dy in ((4, 1), (5, 3)):
+            keys.into(ident, dy, 1)
+            keys.across(dy, 1)
+
+    def handler_5():
+        gate.got_first()
+        for forward in (True, False):
+            pl.when(at.zl == int(forward))(functools.partial(gate_along_z, forward))
         weights_start()
+        wo_middle()
         vals.ring_end(1, 0)
 
-    def handler_5():
-        keys.into(4, 1, 1)
-        keys.across(1, 1)
-        keys.into(5, 3, 1)
-        keys.across(3, 1)
-
-    def handler_7():
+    def handler_6():
         vals.ring_end(4, 1)
         keys.into(6, 2, 1)
         keys.across(2, 1)
-        wo_middle()
 
     def step(t, carry):
         for when, handler in (
-            (0, handler_0), (2, handler_2), (4, handler_4), (5, handler_5), (7, handler_7)
+            (0, handler_0), (2, handler_2), (4, handler_4), (5, handler_5), (6, handler_6)
         ):
 
             @pl.when(t == when)
@@ -403,8 +445,7 @@
         @pl.when(t > 0)
         def _():
             with jax.named_scope("d2d_wait"):
-                keys.from_other(t, chip)
-                vals.from_other(t, chip)
+                keys.both_from_other(t)
 
         @pl.when(early)
         def _():
@@ -426,6 +467,8 @@
     def a_copy(h):
         return remote(a_far.at[h], a_far.at[h], send.at[11], orecv.at[2 + h], sp=at.opposite())
 
+    loads[8].wait()
+    loads[9].wait()
     lanes = lax.broadcasted_iota(jnp.int32, (rows, 128), 1)
     base = 4 - 4 * at.late
     stats = jnp.zeros((rows, 128), F32)
@@ -435,18 +478,13 @@
     stat[...] = stats.T[:8]
     stat_copy().start()
 
-    def weights_on_along_z(forward):
-        up.first_step(forward)
-        gate.second_step(1, forward)
-        gate.second_step(2, forward)
-
     with jax.named_scope("w_first"):
-        gate.got_first()
         for forward in (True, False):
             gate.first_step(forward)
         up.got_first()
         for forward in (True, False):
-            pl.when(at.zl == int(not forward))(functools.partial(weights_on_along_z, forward))
+            up.first_step(forward)
+            pl.when(at.zl == int(not forward))(functools.partial(gate_along_z, forward))
         for j in (1, 2):
             up.along_second(j)
             gate.across(FIRST[j], 0)
@@ -476,9 +514,6 @@
             def _():
                 acc[2 * h] = a
 
-    for forward in (True, False):
-        pl.when(at.zl == int(forward))(functools.partial(weights_on_along_z, forward))
-
     with jax.named_scope("w_second"):
         gate.got_second(0)
         up.got_second(0)
@@ -503,108 +538,123 @@
         a = acc[2 * h]
         square = jnp.mean(a * a, axis=1, keepdims=True)
         n = a * lax.rsqrt(square + EPS) * sub_gain[...] * (1.0 - LAMBDA_INIT)
-        n_loc[:, 256 * h : 256 * h + 256] = n.astype(BF16)
-
-    def n_copy(d, slot, to):
-        return remote(n_loc.at[pl.ds(to * own, own)], n_all.at[slot], send.at[5], xrecv.at[4 + d], tp=to)
-
-    for d in range(1, 4):
-        n_copy(d, x, xs[d]).start()
-    n_all[pl.ds(x, 1)] = n_loc[pl.ds(pl.multiple_of(x * own, own), own), :].reshape(1, own, n_loc.shape[1])
+        n_all[x, 16:, 256 * h : 256 * h + 256] = n.astype(BF16)
+
+    def n_copy(ident, slot, start, size, to):
+        ref = n_all.at[slot, pl.ds(16 + start, size)]
+        return remote(ref, ref, send.at[5], xrecv.at[4 + ident], tp=to)
+
+    @pl.when(sp < 31)
+    def _():
+        for x_to in range(4):
+            n_halo_copy(x, after, x_to).start()
+
+    n_copy(0, x, 0, rows, xs[1]).start()
+    n_copy(1, x, 0, rows, xs[3]).start()
+
     with jax.named_scope("wo_end"):
         wo_end()
     with jax.named_scope("w_third"):
         for j in (1, 2):
-            gate.got_second(j)
+            gate.got_second(j, uneven=True)
             up.got_second(j)
-    with jax.named_scope("n_wait"):
-        for d in range(1, 4):
-            n_copy(d, xs[4 - d], xs[d]).wait_recv()
+    with jax.named_scope("n_middle"):
+        n_copy(0, xs[3], 0, rows, xs[1]).wait_recv()
+        n_copy(2, xs[3], 0, rows // 2, xs[1]).start()
+        n_copy(1, xs[1], 0, rows, xs[3]).wait_recv()
+        n_copy(2, xs[1], rows // 2, rows // 2, xs[3]).start()
+
+    with jax.named_scope("w_fourth"):
+        up.got_second(3)
+        gate.got_second(3)
+
+    @pl.when(sp > 0)
+    def _():
+        with jax.named_scope("halo_wait"):
+            res_copy(before).wait_recv()
+            ref = n_all.at[pl.ds(0, 4), pl.ds(0, 16)]
+            remote(ref, ref, send.at[7], xrecv.at[9], sp=before).wait_recv()
+
+    def project(slots, first):
+        def body(i, carry):
+            cols = pl.ds(pl.multiple_of(i * 256, 256), 256)
+            sums = res[:, cols].astype(F32) if first else mid[:, cols]
+            for slot in slots:
+                sums = sums + jnp.dot(n_all[slot], wo[slot, :, cols], preferred_element_type=F32)
+            mid[:, cols] = sums
+            return carry
+
+        lax.fori_loop(0, mid.shape[1] // 256, body, 0, unroll=2)
+
     with jax.named_scope("wo_wait"):
         wo_wait()
-        loads[7].wait()
-
-    def project(i, carry):
-        cols = pl.ds(pl.multiple_of(i * 256, 256), 256)
-        total = res[:, cols].astype(F32)
-        for j in range(4):
-            total = total + jnp.dot(n_all[j], wo[j, :, cols], preferred_element_type=F32)
-        mid[:, cols] = total
-        return carry
-
     with jax.named_scope("project"):
-        lax.fori_loop(0, mid.shape[1] // 256, project, 0, unroll=True)
-    middle = mid[...]
-    square = jnp.mean(middle * middle, axis=1, keepdims=True)
-
-    def hn_at(slot, start, size):
-        return pl.ds(pl.multiple_of(16 + slot * own + start, 16), size)
-
-    hn[hn_at(x, 0, own), :] = (middle * lax.rsqrt(square + EPS) * norm_gain[...]).astype(BF16)
-
-    def hn_copy(ident, slot, start, size, to):
-        ref = hn.at[hn_at(slot, start, size)]
-        return remote(ref, ref, send.at[6], xrecv.at[8 + ident], tp=to)
-
-    def halo_copy(to):
-        return remote(hn.at[pl.ds(rows, 16)], hn.at[pl.ds(0, 16)], send.at[7], xrecv.at[11], sp=to)
-
-    hn_copy(0, x, 0, own, xs[1]).start()
-    hn_copy(1, x, 0, own, xs[3]).start()
-    with jax.named_scope("w_fourth"):
-        gate.got_second(3)
-        up.got_second(3)
-    with jax.named_scope("hn_middle"):
-        hn_copy(0, xs[3], 0, own, xs[1]).wait_recv()
-        hn_copy(2, xs[3], 0, own // 2, xs[1]).start()
-        hn_copy(1, xs[1], 0, own, xs[3]).wait_recv()
-        hn_copy(2, xs[1], own // 2, own // 2, xs[3]).start()
+        project((x, xs[1], xs[3]), True)
+    with jax.named_scope("n_wait"):
+        n_copy(2, xs[2], 0, rows, xs[1]).wait_recv()
+    with jax.named_scope("project_last"):
+        project((xs[2],), False)
+    for load in loads[10:]:
+        load.wait()
+    with jax.named_scope("norm"):
+        middle = mid[...]
+        square = jnp.mean(middle * middle, axis=1, keepdims=True)
+        hn[...] = (middle * lax.rsqrt(square + EPS) * norm_gain[...]).astype(BF16)
+    feats = hn.shape[1]
+    units = wg.shape[2]
+    row, place = feats // 4, feats // 16
+
+    def gate_part(dz, cols):
+        z = lax.rem(at.z + dz, 4)
+        return jnp.dot(
+            hn[:, pl.ds(pl.multiple_of(z * row, row), row)], wg[pl.ds(z * 8, 8), :, cols].reshape(row, -1),
+            preferred_element_type=F32,
+        )
+
+    def up_part(dy, cols):
+        y = lax.rem(at.y + dy, 4)
+        left = [hn[:, pl.ds(pl.multiple_of(z * row + y * place, place), place)] for z in range(4)]
+        right = [wu[pl.ds(z * 8 + y * 2, 2), :, cols].reshape(place, -1) for z in range(4)]
+        return jnp.dot(
+            jnp.concatenate(left, axis=1), jnp.concatenate(right, axis=0), preferred_element_type=F32
+        )
+
+    def mix(g, taps):
+        return taps[0:1] * pltpu.roll(g, 2, 0) + taps[1:2] * pltpu.roll(g, 1, 0) + taps[2:3] * g
+
+    def feed_most(at_col, width):
+        cols = pl.ds(at_col, width)
+        for i, part_of in enumerate((gate_part, up_part)):
+            pre[i, :, cols] = part_of(0, cols) + part_of(1, cols) + part_of(3, cols)
+
+    def feed_last(at_col, width):
+        cols = pl.ds(at_col, width)
+        mixed = []
+        for i, (part_of, taps) in enumerate(((gate_part, conv_g), (up_part, conv_u))):
+            g = (pre[i, :, cols] + part_of(2, cols)).astype(BF16).astype(F32)
+            mixed.append(mix(g, taps[:, cols])[16:])
+        gc, uc = mixed
+        hid[:, cols] = (gc * (1.0 / (1.0 + jnp.exp(-gc))) * uc).astype(BF16)
+
+    def feed(body):
+        for start in range(0, units, 256):
+            body(start, min(256, units - start))
+
+    with jax.named_scope("w_rest"):
+        gate.from_other(0)
+        up.from_other(0)
+    with jax.named_scope("feed_most"):
+        feed(feed_most)
     with jax.named_scope("w_fifth"):
         for j in range(4):
             gate.got_far(j)
             up.got_far(j)
-    with jax.named_scope("hn_wait"):
-        hn_copy(2, xs[2], 0, own, xs[1]).wait_recv()
-    pl.when(sp < 31)(lambda: halo_copy(after).start())
     with jax.named_scope("w_over"):
-        gate.from_other()
-        up.from_other()
+        gate.from_other(1)
+        up.from_other(1)
         loads[6].wait()
-
-    @pl.when(sp > 0)
-    def _():
-        with jax.named_scope("halo_wait"):
-            halo_copy(before).wait_recv()
-
-    @pl.when(sp == 0)
-    def _():
-        hn[:16, :] = jnp.zeros((16, hn.shape[1]), BF16)
-
-
-    feats = hn.shape[1]
-    units = wg.shape[2]
-
-    def mix(g, taps):
-        return taps[0:1] * pltpu.roll(g, 2, 0) + taps[1:2] * pltpu.roll(g, 1, 0) + taps[2:3] * g
-
-    def feed(at_col, width):
-        cols = pl.ds(at_col, width)
-        mixed = []
-        for w, taps in ((wg, conv_g), (wu, conv_u)):
-            pre = jnp.dot(hn[...], w[:, :, cols].reshape(feats, width), preferred_element_type=F32)
-            mixed.append(mix(pre.astype(BF16).astype(F32), taps[:, cols])[16:])
-        gc, uc = mixed
-        hid[:, cols] = (gc * (1.0 / (1.0 + jnp.exp(-gc))) * uc).astype(BF16)
-
-    def feed_step(i, carry):
-        feed(pl.multiple_of(i * 256, 256), 256)
-        return carry
-
-    whole = units // 256
     with jax.named_scope("feed"):
-        lax.fori_loop(0, whole, feed_step, 0, unroll=True)
-        if units % 256:
-            feed(whole * 256, units % 256)
+        feed(feed_last)
 
     chunks = part.shape[2] // 512
     side = own // 2
@@ -615,13 +665,17 @@
     def relay_copy(s, i, to):
         return remote(
             part.at[xs[2], pl.ds(s * side, side), cols_of(i)], relay.at[s, :, cols_of(i)],
-            send.at[8], precv.at[0, s, i], tp=to,
+            send.at[8], precv.at[0, i], tp=to,
         )
 
     def part_copy(s, i, to):
         return remote(
-            part.at[to, :, cols_of(i)], parts.at[s, :, cols_of(i)], send.at[8], precv.at[1, s, i], tp=to
+            part.at[to, :, cols_of(i)], parts.at[s, :, cols_of(i)], send.at[8], precv.at[1, i], tp=to
         )
+
+    def arrived(buf, which, i):
+        ref = buf.at[:, :, cols_of(i)]
+        remote(ref, ref, send.at[8], precv.at[which, i], tp=xs[1]).wait_recv()
 
     def lower(i, carry):
         cols = cols_of(i)
@@ -636,27 +690,13 @@
 
     def pass_on(i, carry):
         cols = cols_of(i)
+        arrived(relay, 0, i)
         for s, to in ((0, xs[1]), (1, xs[3])):
-            relay_copy(s, i, to).wait_recv()
             half = pl.ds(s * side, side)
-            total = part[to, half, cols].astype(F32) + relay[s, :, cols].astype(F32)
-            part[to, half, cols] = total.astype(BF16)
+            both = part[to, half, cols].astype(F32) + relay[s, :, cols].astype(F32)
+            part[to, half, cols] = both.astype(BF16)
             part_copy(s, i, to).start()
         return carry
-
-    with jax.named_scope("pass_on"):
-        lax.fori_loop(0, chunks, pass_on, 0)
-
-    def finish(i, carry):
-        cols = cols_of(i)
-        for s, to in ((0, xs[1]), (1, xs[3])):
-            part_copy(s, i, to).wait_recv()
-        total = parts[0, :, cols].astype(F32) + parts[1, :, cols].astype(F32) + part[x, :, cols].astype(F32)
-        out[:, cols] = (mid[:, cols] + total).astype(BF16)
-        return carry
-
-    with jax.named_scope("finish"):
-        lax.fori_loop(0, chunks, finish, 0)
 
     def sent(ref, which):
         remote(ref, ref, send.at[which], xrecv.at[0], sp=other).wait_send()
@@ -665,11 +705,13 @@
         for gather in (keys, vals, gate, up):
             gather.drain()
         sent(wo.at[pl.ds(0, 3)], 4)
-        sent(n_all.at[pl.ds(0, 3)], 5)
-        sent(hn.at[pl.ds(0, 3 * own)], 6)
-        pl.when(sp < 31)(lambda: halo_copy(after).wait_send())
-        sent(hn.at[pl.ds(0, 3 * own)], 8)
+        sent(n_all.at[pl.ds(0, 3), pl.ds(0, rows)], 5)
         stat_copy().wait_send()
+
+        @pl.when(sp < 31)
+        def _():
+            sent(hn.at[pl.ds(0, 16)], 6)
+            sent(n_all.at[pl.ds(0, 4), pl.ds(0, 16)], 7)
 
         @pl.when(late)
         def _():
@@ -678,6 +720,25 @@
         @pl.when(early)
         def _():
             sent(a_far, 11)
+
+    with jax.named_scope("pass_on"):
+        lax.fori_loop(0, chunks, pass_on, 0)
+
+    def finish(i, carry):
+        cols = cols_of(i)
+        arrived(parts, 1, i)
+        sums = parts[0, :, cols].astype(F32) + parts[1, :, cols].astype(F32) + part[x, :, cols].astype(F32)
+        middle = mid[pl.ds(pl.multiple_of(16 + x * own, 16), own), cols]
+        ended[:, cols] = (middle + sums).astype(BF16)
+        pltpu.make_async_copy(ended.at[:, cols], out.at[:, cols], lsem.at[i]).start()
+        return carry
+
+    with jax.named_scope("finish"):
+        lax.fori_loop(0, chunks, finish, 0)
+
+    sent(hn.at[pl.ds(0, 3 * own)], 8)
+    for i in range(chunks):
+        pltpu.make_async_copy(ended.at[:, cols_of(i)], out.at[:, cols_of(i)], lsem.at[i]).wait()
 
 
 def local(
@@ -692,15 +753,18 @@
     maps = queries.shape[1] * 2
     places = 32
     hbm = pl.BlockSpec(memory_space=pl.ANY)
-    vmem = pl.BlockSpec(memory_space=pltpu.VMEM)
-    smem = pl.BlockSpec(memory_space=pltpu.SMEM)
     dma = pltpu.SemaphoreType.DMA
     call = pl.pallas_call(
         kernel,
         out_shape=jax.ShapeDtypeStruct((own, d), BF16),
-        in_specs=[smem] + [vmem] * 4 + [hbm] * 8,
-        out_specs=vmem,
+        in_specs=[hbm] * 13,
+        out_specs=hbm,
         scratch_shapes=[
+            pltpu.SMEM(lambda_head.shape, F32),
+            pltpu.VMEM((1, *sub_gain.shape), F32),
+            pltpu.VMEM((1, d), F32),
+            pltpu.VMEM(conv_gate.shape, F32),
+            pltpu.VMEM(conv_up.shape, F32),
             pltpu.VMEM(queries.shape, BF16),
             pltpu.VMEM(key_rows.shape, BF16),
             pltpu.VMEM(values.shape, BF16),
@@ -711,23 +775,24 @@
             pltpu.VMEM((places, w_gate.shape[0], units), BF16),
             pltpu.VMEM((4, *w_out.shape), BF16),
             pltpu.VMEM(w_down.shape, BF16),
-            pltpu.VMEM((own, d), BF16),
+            pltpu.VMEM((rows + 16, d), BF16),
             pltpu.VMEM((2 * maps, rows, 128), F32),
             pltpu.VMEM((2 * maps, rows, 128), F32),
             pltpu.VMEM((2 * maps, rows, values.shape[2]), F32),
             pltpu.VMEM((2, rows, values.shape[2]), BF16),
             pltpu.VMEM((8, rows), F32),
             pltpu.VMEM((8, rows), F32),
-            pltpu.VMEM((rows, heads_wide), BF16),
-            pltpu.VMEM((4, own, heads_wide), BF16),
-            pltpu.VMEM((own, d), F32),
+            pltpu.VMEM((4, rows + 16, heads_wide), BF16),
+            pltpu.VMEM((rows + 16, d), F32),
             pltpu.VMEM((rows + 16, d), BF16),
+            pltpu.VMEM((2, rows + 16, units), F32),
             pltpu.VMEM((rows, units), BF16),
             pltpu.VMEM((4, own, d), BF16),
             pltpu.VMEM((2, own // 2, d), BF16),
             pltpu.VMEM((2, own, d), BF16),
-            dma((8,)), dma((12,)), dma((2, 7)), dma((2, 8)), dma((2, 15)), dma((2,)), dma((4,)), dma((12,)),
-            dma((2, 2, d // 512)),
+            pltpu.VMEM((own, d), BF16),
+            dma((13,)), dma((12,)), dma((2, 7)), dma((8,)), dma((2, 15)), dma((2, 2)), dma((4,)), dma((10,)),
+            dma((2, d // 512)),
         ],
         compiler_params=pltpu.CompilerParams(
             collective_id=0, has_side_effects=True, vmem_limit_bytes=67043328

time: 99.6 us -> 91.7 us (0.921)
  the two profiles are of different devices: /device:TPU:98 before, /device:TPU:1 now
where the time goes in v3:
time: 91.7 us; the launch traced here: 90.4 us
  Pallas kernels  88.7 us (97%)
  local copies, waits for them, and re-layouts  1.67 us (2%)
    pallas_call x1, Pallas kernels, local(): call(lambda_head, sub_gain[None], norm_gain[None], conv_gate, conv_up, qu...  88.7 us

profile of v3, /device:TPU:1, one launch (start us, length us, event | category | flops | bytes accessed | tf_op | source)
XLA Modules:
  0.0 90.4 jit_solution(8146217647701584201)
XLA Ops:
  0.0 88.7 %shard_map.127 = bf16[64,2048]{1,0:T(8,128)(2,1)} custom-call(f32[2]{0:T(128)} %lam_in.1, f32[1,256]{1,0:T(1,128)} %bitcast.3, f32[1,2048]{1,0:T(1,128)} %bitcast.2, f32[3,1408]{1,0:T(4,128)} %conv_g_in.1, f32[3,1408]{1,0:T(4,128)} %conv_u_in.1, bf16[256,2,2,128]{3,2,1,0:T(2,128)(2,1)} %q_in.1, bf16[256,2,2,128]{3,2,1,0:T(2,128)(2,1)} %k_in.1, ...), custom_call_target="tpu_custom_call" | custom-call | tf_op jit(solution)/shard_map/pallas_call | solution.py:801
  88.7 1.7 %copy.15 = bf16[64,2048]{1,0:T(8,128)(2,1)} copy(bf16[64,2048]{1,0:T(8,128)(2,1)} %shard_map.127) | data formatting | bytes 524288

commit v4 on v3

--- a/solution.py
+++ b/solution.py
@@ -210,7 +210,7 @@
     out,
     lam, sub_gain, norm_gain, conv_g, conv_u, q_raw, k_raw, v_raw, q, kbuf, vbuf, wg, wu, wo, wd, res,
     m_s, l_s, acc, a_far, stat, stat_far, n_all, mid, hn, pre, hid, part, relay, parts, ended,
-    lsem, send, krecv, kdrecv, wrecv, drecv, orecv, xrecv, precv,
+    lsem, send, krecv, kdrecv, wrecv, drecv, orecv, nrecv, xrecv, precv,
 ):
     at = Where()
     x, sp, core, other = at.x, at.sp, at.core, at.other
@@ -416,13 +416,25 @@
             keys.into(ident, dy, 1)
             keys.across(dy, 1)
 
+    def up_on(forward):
+        up.into(0 if forward else 1, 1 if forward else 3, 0)
+        up.first_step(forward)
+        up.along_second(1 if forward else 2)
+
     def handler_5():
         gate.got_first()
         for forward in (True, False):
             pl.when(at.zl == int(forward))(functools.partial(gate_along_z, forward))
         weights_start()
+        vals.ring_end(1, 0)
+        for forward in (True, False):
+            gate.first_step(forward)
+        for forward in (True, False):
+            pl.when(at.zl == int(not forward))(functools.partial(up_on, forward))
+            pl.when(at.zl == int(not forward))(functools.partial(gate_along_z, forward))
+        gate.across(FIRST[1], 0)
+        gate.across(FIRST[2], 0)
         wo_middle()
-        vals.ring_end(1, 0)
 
     def handler_6():
         vals.ring_end(4, 1)
@@ -451,6 +463,17 @@
         def _():
             with jax.named_scope("far_block"):
                 block(1, chip, False)
+
+        @pl.when((chip < mine) & (late | (t < 4)))
+        def _():
+            with jax.named_scope("block"):
+                block(0, chip, False)
+
+        return carry
+
+    def own_step(t, carry):
+        dy, zo = (pick(t, [d[i] for d in HALF_ORDER]) for i in (0, 1))
+        chip = at.half_chip(dy, zo)
 
         @pl.when(chip < mine)
         def _():
@@ -480,14 +503,7 @@
 
     with jax.named_scope("w_first"):
         for forward in (True, False):
-            gate.first_step(forward)
-        up.got_first()
-        for forward in (True, False):
-            up.first_step(forward)
-            pl.when(at.zl == int(not forward))(functools.partial(gate_along_z, forward))
-        for j in (1, 2):
-            up.along_second(j)
-            gate.across(FIRST[j], 0)
+            pl.when(at.zl == int(forward))(functools.partial(up_on, forward))
 
     with jax.named_scope("stat_wait"):
         stat_copy().wait_recv()
@@ -514,12 +530,20 @@
             def _():
                 acc[2 * h] = a
 
+    @pl.when(early)
+    def _():
+        lax.fori_loop(4, 8, own_step, 0)
+
     with jax.named_scope("w_second"):
         gate.got_second(0)
         up.got_second(0)
         gate.got_opposite()
         up.got_opposite()
 
+    def n_copy(ident, h, slot, start, size, to):
+        ref = n_all.at[slot, pl.ds(16 + start, size), pl.ds(256 * h, 256)]
+        return remote(ref, ref, send.at[5], nrecv.at[h, ident], tp=to)
+
     for h in range(2):
 
         @pl.when(late)
@@ -539,18 +563,13 @@
         square = jnp.mean(a * a, axis=1, keepdims=True)
         n = a * lax.rsqrt(square + EPS) * sub_gain[...] * (1.0 - LAMBDA_INIT)
         n_all[x, 16:, 256 * h : 256 * h + 256] = n.astype(BF16)
-
-    def n_copy(ident, slot, start, size, to):
-        ref = n_all.at[slot, pl.ds(16 + start, size)]
-        return remote(ref, ref, send.at[5], xrecv.at[4 + ident], tp=to)
+        n_copy(0, h, x, 0, rows, xs[1]).start()
+        n_copy(1, h, x, 0, rows, xs[3]).start()
 
     @pl.when(sp < 31)
     def _():
         for x_to in range(4):
             n_halo_copy(x, after, x_to).start()
-
-    n_copy(0, x, 0, rows, xs[1]).start()
-    n_copy(1, x, 0, rows, xs[3]).start()
 
     with jax.named_scope("wo_end"):
         wo_end()
@@ -559,10 +578,11 @@
             gate.got_second(j, uneven=True)
             up.got_second(j)
     with jax.named_scope("n_middle"):
-        n_copy(0, xs[3], 0, rows, xs[1]).wait_recv()
-        n_copy(2, xs[3], 0, rows // 2, xs[1]).start()
-        n_copy(1, xs[1], 0, rows, xs[3]).wait_recv()
-        n_copy(2, xs[1], rows // 2, rows // 2, xs[3]).start()
+        for h in range(2):
+            n_copy(0, h, xs[3], 0, rows, xs[1]).wait_recv()
+            n_copy(2, h, xs[3], 0, rows // 2, xs[1]).start()
+            n_copy(1, h, xs[1], 0, rows, xs[3]).wait_recv()
+            n_copy(2, h, xs[1], rows // 2, rows // 2, xs[3]).start()
 
     with jax.named_scope("w_fourth"):
         up.got_second(3)
@@ -591,7 +611,8 @@
     with jax.named_scope("project"):
         project((x, xs[1], xs[3]), True)
     with jax.named_scope("n_wait"):
-        n_copy(2, xs[2], 0, rows, xs[1]).wait_recv()
+        for h in range(2):
+            n_copy(2, h, xs[2], 0, rows, xs[1]).wait_recv()
     with jax.named_scope("project_last"):
         project((xs[2],), False)
     for load in loads[10:]:
@@ -634,7 +655,7 @@
             g = (pre[i, :, cols] + part_of(2, cols)).astype(BF16).astype(F32)
             mixed.append(mix(g, taps[:, cols])[16:])
         gc, uc = mixed
-        hid[:, cols] = (gc * (1.0 / (1.0 + jnp.exp(-gc))) * uc).astype(BF16)
+        hid[:, cols] = (gc * (0.5 + 0.5 * jnp.tanh(0.5 * gc)) * uc).astype(BF16)
 
     def feed(body):
         for start in range(0, units, 256):
@@ -791,7 +812,7 @@
             pltpu.VMEM((2, own // 2, d), BF16),
             pltpu.VMEM((2, own, d), BF16),
             pltpu.VMEM((own, d), BF16),
-            dma((13,)), dma((12,)), dma((2, 7)), dma((8,)), dma((2, 15)), dma((2, 2)), dma((4,)), dma((10,)),
+            dma((13,)), dma((12,)), dma((2, 7)), dma((8,)), dma((2, 15)), dma((2, 2)), dma((4,)), dma((2, 3)), dma((10,)),
             dma((2, d // 512)),
         ],
         compiler_params=pltpu.CompilerParams(

time: 91.7 us -> 88 us (0.960); the launches traced: 90.4 us -> 87.9 us
  Pallas kernels: 88.7 us -> 86.2 us
    pallas_call x1, Pallas kernels: 88.7 us -> 86.2 us  [local(): call(lambda_head, sub_gain[None], norm_gain[None], conv_gate, conv_up, qu...]
where the time goes in v4:
time: 88 us; the launch traced here: 87.9 us
  Pallas kernels  86.2 us (98%)
  local copies, waits for them, and re-layouts  1.67 us (2%)
    pallas_call x1, Pallas kernels, local(): call(lambda_head, sub_gain[None], norm_gain[None], conv_gate, conv_up, qu...  86.2 us

profile of v4, /device:TPU:1, one launch (start us, length us, event | category | flops | bytes accessed | tf_op | source)
XLA Modules:
  0.0 87.9 jit_solution(18380051163159535846)
XLA Ops:
  0.0 86.2 %shard_map.127 = bf16[64,2048]{1,0:T(8,128)(2,1)} custom-call(f32[2]{0:T(128)} %lam_in.1, f32[1,256]{1,0:T(1,128)} %bitcast.3, f32[1,2048]{1,0:T(1,128)} %bitcast.2, f32[3,1408]{1,0:T(4,128)} %conv_g_in.1, f32[3,1408]{1,0:T(4,128)} %conv_u_in.1, bf16[256,2,2,128]{3,2,1,0:T(2,128)(2,1)} %q_in.1, bf16[256,2,2,128]{3,2,1,0:T(2,128)(2,1)} %k_in.1, ...), custom_call_target="tpu_custom_call" | custom-call | tf_op jit(solution)/shard_map/pallas_call | solution.py:822
  86.2 1.7 %copy.15 = bf16[64,2048]{1,0:T(8,128)(2,1)} copy(bf16[64,2048]{1,0:T(8,128)(2,1)} %shard_map.127) | data formatting | bytes 524288

commit v5 on v4

--- a/solution.py
+++ b/solution.py
@@ -277,8 +277,8 @@
         q_copy().start()
 
     def weights_along_z(forward):
+        up.start_along("f", forward)
         gate.start_along("g", forward)
-        up.start_along("f", forward)
 
     loads[4].wait()
     loads[5].wait()
@@ -661,13 +661,17 @@
         for start in range(0, units, 256):
             body(start, min(256, units - start))
 
+    with jax.named_scope("w_far"):
+        for j in (0, 1):
+            gate.got_far(j)
+            up.got_far(j)
     with jax.named_scope("w_rest"):
         gate.from_other(0)
         up.from_other(0)
     with jax.named_scope("feed_most"):
         feed(feed_most)
     with jax.named_scope("w_fifth"):
-        for j in range(4):
+        for j in (2, 3):
             gate.got_far(j)
             up.got_far(j)
     with jax.named_scope("w_over"):

time: 88 us -> 87 us (0.989)
  Pallas kernels: 86.2 us -> 85.2 us
    pallas_call x1, Pallas kernels: 86.2 us -> 85.2 us  [local(): call(lambda_head, sub_gain[None], norm_gain[None], conv_gate, conv_up, qu...]
where the time goes in v5:
time: 87 us; the launch traced here: 86.9 us
  Pallas kernels  85.2 us (98%)
  local copies, waits for them, and re-layouts  1.67 us (2%)
    pallas_call x1, Pallas kernels, local(): call(lambda_head, sub_gain[None], norm_gain[None], conv_gate, conv_up, qu...  85.2 us

profile of v5, /device:TPU:1, one launch (start us, length us, event | category | flops | bytes accessed | tf_op | source)
XLA Modules:
  0.0 86.9 jit_solution(16746861175899038606)
XLA Ops:
  0.0 85.2 %shard_map.127 = bf16[64,2048]{1,0:T(8,128)(2,1)} custom-call(f32[2]{0:T(128)} %lam_in.1, f32[1,256]{1,0:T(1,128)} %bitcast.3, f32[1,2048]{1,0:T(1,128)} %bitcast.2, f32[3,1408]{1,0:T(4,128)} %conv_g_in.1, f32[3,1408]{1,0:T(4,128)} %conv_u_in.1, bf16[256,2,2,128]{3,2,1,0:T(2,128)(2,1)} %q_in.1, bf16[256,2,2,128]{3,2,1,0:T(2,128)(2,1)} %k_in.1, ...), custom_call_target="tpu_custom_call" | custom-call | tf_op jit(solution)/shard_map/pallas_call | solution.py:826
  85.2 1.7 %copy.15 = bf16[64,2048]{1,0:T(8,128)(2,1)} copy(bf16[64,2048]{1,0:T(8,128)(2,1)} %shard_map.127) | data formatting | bytes 524288

commit v6 on v5

--- a/solution.py
+++ b/solution.py
@@ -657,23 +657,26 @@
         gc, uc = mixed
         hid[:, cols] = (gc * (0.5 + 0.5 * jnp.tanh(0.5 * gc)) * uc).astype(BF16)
 
-    def feed(body):
-        for start in range(0, units, 256):
+    def feed(body, first=0, last=units):
+        for start in range(first, last, 256):
             body(start, min(256, units - start))
 
-    with jax.named_scope("w_far"):
-        for j in (0, 1):
+    def far(*places):
+        for j in places:
             gate.got_far(j)
             up.got_far(j)
+
+    with jax.named_scope("w_far"):
+        far(0, 1)
     with jax.named_scope("w_rest"):
         gate.from_other(0)
         up.from_other(0)
     with jax.named_scope("feed_most"):
-        feed(feed_most)
+        feed(feed_most, last=768)
+        far(2)
+        feed(feed_most, first=768)
     with jax.named_scope("w_fifth"):
-        for j in (2, 3):
-            gate.got_far(j)
-            up.got_far(j)
+        far(3)
     with jax.named_scope("w_over"):
         gate.from_other(1)
         up.from_other(1)

time: 87 us -> 86.7 us (level)
  no operation moved by 1% of the time
where the time goes in v6:
time: 86.7 us; the launch traced here: 86.5 us
  Pallas kernels  84.8 us (98%)
  local copies, waits for them, and re-layouts  1.67 us (2%)
    pallas_call x1, Pallas kernels, local(): call(lambda_head, sub_gain[None], norm_gain[None], conv_gate, conv_up, qu...  84.8 us

profile of v6, /device:TPU:1, one launch (start us, length us, event | category | flops | bytes accessed | tf_op | source)
XLA Modules:
  0.0 86.5 jit_solution(13474575902540355195)
XLA Ops:
  0.0 84.8 %shard_map.127 = bf16[64,2048]{1,0:T(8,128)(2,1)} custom-call(f32[2]{0:T(128)} %lam_in.1, f32[1,256]{1,0:T(1,128)} %bitcast.3, f32[1,2048]{1,0:T(1,128)} %bitcast.2, f32[3,1408]{1,0:T(4,128)} %conv_g_in.1, f32[3,1408]{1,0:T(4,128)} %conv_u_in.1, bf16[256,2,2,128]{3,2,1,0:T(2,128)(2,1)} %q_in.1, bf16[256,2,2,128]{3,2,1,0:T(2,128)(2,1)} %k_in.1, ...), custom_call_target="tpu_custom_call" | custom-call | tf_op jit(solution)/shard_map/pallas_call | solution.py:829
  84.9 1.7 %copy.15 = bf16[64,2048]{1,0:T(8,128)(2,1)} copy(bf16[64,2048]{1,0:T(8,128)(2,1)} %shard_map.127) | data formatting | bytes 524288
